TPU v7x, 256 devices: a whole 4x4x8 slice. The times are simulated.
256 devices in a mesh: dp: 4 (over x), kv: 32 (over z, y), tp: 2 (over core).
Axes of the slice: x: 4, y: 4, z: 8, core: 2. Of those that a mesh axis runs over, the one named last changes fastest.
Arguments:
- tokens: bfloat16 [4, 16384, 1024], P('dp', ('kv', 'tp')), may hold values from -6 to 6
- w_query: bfloat16 [1024, 1024], P(None, 'tp'), may hold values from -0.1875 to 0.1875
- w_key: bfloat16 [1024, 256], P(None, 'tp'), may hold values from -0.1875 to 0.1875
- w_value: bfloat16 [1024, 256], P(None, 'tp'), may hold values from -0.1875 to 0.1875
- w_out: bfloat16 [1024, 1024], P('tp'), may hold values from -0.1875 to 0.1875
- chosen: int32 [4, 256, 15], P('dp', 'kv'), may hold values from -1 to 254, as said below
Outputs:
- normed: bfloat16 [4, 16384, 1024], P('dp', ('kv', 'tp'))
- logsums: float32 [4, 16384, 16], P('dp', 'kv', 'tp')
Inputs may be any that keep to these rules, and one draw needn't show every extreme that they name: Each entry of chosen[s, c] is -1 or a block below c; entries of a row that are not -1 differ. Within a sequence, the 15 times 8 entries of the query blocks of one aligned run of 8 blocks name at most 4 different blocks inside any one aligned run, and some run pair reaches exactly 4.
All inputs are finite; a program needn't handle non-finite values.
Results may differ from a plain program's by a relative error of at most 0.0085.
Values may be sent and summed in bfloat16 or wider, within the bound.
A program may use at most 64 MiB of HBM per device.

v0:
```python
import functools
import math

import jax
import jax.numpy as jnp
import numpy as np
from jax import lax
from jax.experimental import pallas as pl
from jax.experimental.pallas import tpu as pltpu
from jax.sharding import PartitionSpec as P

HEAD_DIM = 64
BLK = 64
PICK = 15
THETA_BASE = 10000.0
NEGATIVE = -1e30
EPSILON = 1e-06
MESH = pl.DeviceIdType.MESH
BF = jnp.bfloat16
F32 = jnp.float32
EXPONENT = math.log2(math.e) / math.sqrt(HEAD_DIM)
NY = 4
NZ = 8


def rotary_tables(rows, bases):
    half = HEAD_DIM // 2
    freq = THETA_BASE ** (-np.arange(half, dtype=np.float64) / half)
    freq = np.tile(freq, 128 // half)[None, :]
    offset = np.arange(rows, dtype=np.float64)[:, None] * freq
    base = np.arange(bases, dtype=np.float64)[:, None] * rows * freq
    return [
        np.asarray(a, np.float32)
        for a in (np.cos(offset), np.sin(offset), np.cos(base), np.sin(base))
    ]


def kernel(
    cr_ref, sr_ref, cb_ref, sb_ref, tok_hbm, wq_hbm, wk_hbm, wv_hbm, wo_hbm, chosen_ref,
    out_ref, ls_ref,
    tok, wq, wk, wv, wo, cosine, sine, kvs, kv_all, qs, q_all, ch_all, ch_smem,
    kg, vt, scores, probs, att_out, att_all, ls_out, acc,
    load_sem, w_send, w_recv, ky_send, ky_recv, up_send, up_recv, dn_send, dn_recv,
    pt_send, pt_recv, q_send, q_recv, c_send, c_recv, a_send, a_recv, l_send, l_recv,
):
    kv = lax.axis_index("kv")
    t = lax.axis_index("tp")
    z, y = kv // NY, kv % NY
    other = 1 - t

    def row_peer(k):
        return z * NY + lax.rem(y + k, NY)

    def chunk(zz, yy):
        return pl.ds(((zz * NY + yy) * 2 + t) * 4, 4)

    def remote(src, dst, send, recv, kv_to, tp_to):
        copy = pltpu.make_async_remote_copy(
            src_ref=src, dst_ref=dst, send_sem=send, recv_sem=recv,
            device_id={"kv": kv_to, "tp": tp_to}, device_id_type=MESH,
        )
        copy.start()
        return copy

    loads = [
        pltpu.make_async_copy(tok_hbm, tok, load_sem.at[0]),
        pltpu.make_async_copy(wk_hbm, wk.at[t], load_sem.at[1]),
        pltpu.make_async_copy(wv_hbm, wv.at[t], load_sem.at[2]),
        pltpu.make_async_copy(wq_hbm, wq.at[t], load_sem.at[3]),
        pltpu.make_async_copy(wo_hbm, wo.at[t], load_sem.at[4]),
    ]
    for load in loads:
        load.start()

    barrier = pltpu.get_barrier_semaphore()
    peers = [(row_peer(k), tt) for k in range(1, NY) for tt in (t, other)]
    peers += [(kv, other)]
    z_up = lax.rem(z + 1, NZ) * NY + y
    z_dn = lax.rem(z + NZ - 1, NZ) * NY + y
    peers += [(z_up, t), (z_dn, t)]
    for kv_to, tp_to in peers:
        pl.semaphore_signal(
            barrier, inc=1, device_id={"kv": kv_to, "tp": tp_to}, device_id_type=MESH
        )
    pl.semaphore_wait(barrier, len(peers))

    sent = []
    halves = [
        remote(wk_hbm, wk.at[t], w_send.at[0], w_recv.at[0], kv, other),
        remote(wv_hbm, wv.at[t], w_send.at[1], w_recv.at[1], kv, other),
        remote(wq_hbm, wq.at[t], w_send.at[2], w_recv.at[2], kv, other),
        remote(wo_hbm, wo.at[t], w_send.at[3], w_recv.at[3], kv, other),
    ]
    sent += halves

    ch_all[0] = chosen_ref[...]
    picks = [
        remote(chosen_ref, ch_all.at[NY - k], c_send.at[k], c_recv.at[NY - k], row_peer(k), t)
        for k in range(1, NY)
    ]
    sent += picks

    lane = lax.broadcasted_iota(jnp.int32, (BLK, 128), 1)
    left = lane < BLK
    wide = lax.broadcasted_iota(jnp.int32, (4 * BLK, 128), 1)
    first = lax.rem(wide, HEAD_DIM) < HEAD_DIM // 2

    base = kv * 2 + t
    cb, sb = cb_ref[pl.ds(base, 1), :], sb_ref[pl.ds(base, 1), :]
    cr, sr = cr_ref[...], sr_ref[...]
    cosine[...] = cb * cr - sb * sr
    turned = sb * cr + cb * sr
    sine[...] = jnp.where(first, -turned, turned)

    def rotate(x):
        swapped = jnp.where(first, pltpu.roll(x, 96, 1), pltpu.roll(x, 32, 1))
        return x * cosine[...] + swapped * sine[...]

    def project_kv(half):
        tokens = tok[...]
        keys = jnp.dot(tokens, wk[half], preferred_element_type=F32).astype(BF).astype(F32)
        keys = rotate(keys)
        values = jnp.dot(tokens, wv[half], preferred_element_type=F32)
        values_t = values.T
        keys_swapped = pltpu.roll(keys, 64, 1)
        for e in range(2):
            k_e = keys if e == 0 else keys_swapped
            for j in range(4):
                v_e = values_t[e * 64 : e * 64 + 64, (j // 2) * 128 : (j // 2) * 128 + 128]
                if j % 2 == 0:
                    v_e = pltpu.roll(v_e, 64, 1)
                kvs[2 * half + e, j] = jnp.where(left, k_e[j * 64 : j * 64 + 64], v_e).astype(BF)

    for load in loads[:3]:
        load.wait()
    project_kv(t)
    for copy in halves[:2]:
        copy.wait_recv()
    project_kv(other)

    mine = pltpu.make_async_copy(kvs.at[y], kv_all.at[chunk(z, y)], load_sem.at[5])
    mine.start()
    gathered = [None] * NY
    for k in (1, 3, 2):
        gathered[NY - k] = remote(
            kvs.at[lax.rem(y + k, NY)], kv_all.at[chunk(z, y)],
            ky_send.at[k], ky_recv.at[NY - k], row_peer(k), t,
        )
    sent += gathered[1:]

    ups, downs, partner = {}, {}, {}

    def pass_on(src, zz, k, up=None, down=None, rel=0):
        place = kv_all.at[chunk(zz, lax.rem(y + k, NY))]
        src = place if src is None else src
        if up is not None:
            ups[up, k] = remote(src, place, up_send.at[up, k], up_recv.at[up, k], z_up, t)
        if down is not None:
            downs[down, k] = remote(src, place, dn_send.at[down, k], dn_recv.at[down, k], z_dn, t)
        partner[rel, k] = remote(src, place, pt_send.at[rel, k], pt_recv.at[rel, k], kv, other)

    pass_on(kvs.at[y], z, 0, up=0, down=0, rel=0)

    def project_q(half):
        tokens = tok[...]
        full = jnp.dot(tokens, wq[half], preferred_element_type=F32)
        for n in range(4):
            x = full[:, n * 128 : n * 128 + 128].astype(BF).astype(F32)
            qs[2 * half + n // 2, :, (n % 2) * 128 : (n % 2) * 128 + 128] = rotate(x).astype(BF)

    loads[3].wait()
    project_q(t)
    for k in (1, 3):
        gathered[k].wait_recv()
        pass_on(None, z, k, up=0, down=0, rel=0)
    halves[2].wait_recv()
    project_q(other)
    gathered[2].wait_recv()
    pass_on(None, z, 2, up=0, down=0, rel=0)

    own_q = pltpu.make_async_copy(qs.at[y], q_all.at[0], load_sem.at[6])
    own_q.start()
    queries = [None] * NY
    for k in (2, 1, 3):
        queries[NY - k] = remote(
            qs.at[lax.rem(y + k, NY)], q_all.at[NY - k],
            q_send.at[k], q_recv.at[NY - k], row_peer(k), t,
        )
    sent += queries[1:]

    order = (0, 1, 3, 2)
    for s in range(1, NZ // 2 + 1):
        last = s == NZ // 2
        for k in order:
            if not last or k in (0, 1):
                ups[s - 1, k].wait_recv()
                more = s + 1 < NZ // 2 or (s + 1 == NZ // 2 and k in (0, 1))
                pass_on(
                    None, lax.rem(z + NZ - s, NZ), k, up=s if more else None, rel=NZ - s
                )
            if not last or k in (2, 3):
                downs[s - 1, k].wait_recv()
                more = s + 1 < NZ // 2 or (s + 1 == NZ // 2 and k in (2, 3))
                pass_on(None, lax.rem(z + s, NZ), k, down=s if more else None, rel=s)

    for copy in picks:
        copy.wait_recv()
    to_smem = pltpu.make_async_copy(ch_all, ch_smem, load_sem.at[7])
    to_smem.start()
    to_smem.wait()
    own_q.wait()
    mine.wait()
    for k in range(1, NY):
        queries[k].wait_recv()
    for copy in partner.values():
        copy.wait_recv()

    key_pos = lax.broadcasted_iota(jnp.int32, (BLK, 4 * BLK), 0)
    query_pos = lax.rem(lax.broadcasted_iota(jnp.int32, (BLK, 4 * BLK), 1), BLK)
    causal = key_pos <= query_pos

    def attend(k, jb):
        rows = pl.ds(pl.multiple_of(jb * BLK, BLK), BLK)
        heads = []
        for n in range(2):
            x = q_all[k, rows, n * 128 : n * 128 + 128].astype(F32)
            heads.append(jnp.where(left, x, 0.0))
            heads.append(jnp.where(left, pltpu.roll(x, 64, 1), 0.0))
        q2 = jnp.concatenate(heads, axis=0).astype(BF)
        own = (z * NY + lax.rem(y + k, NY)) * 8 + t * 4 + jb
        bias = []
        block = None
        for j in range(PICK + 1):
            previous = block
            if j < PICK:
                pick = ch_smem[k, t * 4 + jb, j]
                bias.append(jnp.where(pick < 0, NEGATIVE, 0.0).astype(F32))
                block = kv_all[jnp.maximum(pick, 0)]
            else:
                bias.append(None)
                block = kv_all[own]
            kg[j * BLK : j * BLK + BLK, :] = block
            if j % 2 == 1:
                pair = jnp.where(
                    left, pltpu.roll(previous.astype(F32), 64, 1), block.astype(F32)
                )
                vt[:, (j // 2) * 128 : (j // 2) * 128 + 128] = pair.astype(BF)
        scores[...] = lax.dot_general(
            kg[...], q2, (((1,), (1,)), ((), ())), preferred_element_type=F32
        )
        tail = jnp.where(causal, scores[PICK * BLK :, :], NEGATIVE)
        top = jnp.max(tail, axis=0, keepdims=True)
        for j in range(PICK):
            here = jnp.max(scores[j * BLK : j * BLK + BLK, :], axis=0, keepdims=True)
            top = jnp.maximum(top, here + bias[j])
        total = jnp.zeros((1, 4 * BLK), F32)
        for j in range(PICK + 1):
            s = tail if j == PICK else scores[j * BLK : j * BLK + BLK, :]
            shift = top if j == PICK else top - bias[j]
            p = jnp.exp2((s - shift) * EXPONENT)
            total = total + jnp.sum(p, axis=0, keepdims=True)
            probs[j * BLK : j * BLK + BLK, :] = p.astype(BF)
        mixed = jnp.dot(vt[...], probs[...], preferred_element_type=F32)
        mixed = mixed * (1.0 / total)
        turned_back = mixed.T
        parts = [turned_back[h * BLK : h * BLK + BLK] for h in range(4)]
        att_out[k, rows, :] = jnp.concatenate(parts, axis=1).astype(BF)
        ls_out[k, pl.ds(jb, 1), :] = top * HEAD_DIM**-0.5 + jnp.log(total)

    back, logs = {}, {}
    to_self = y // 2 == t
    for k in (2, 1, 3, 0):
        @pl.loop(0, 4)
        def _(jb):
            attend(k, jb)

        if k > 0:
            back[NY - k] = remote(
                att_out.at[k], att_all.at[NY - k], a_send.at[k], a_recv.at[NY - k],
                row_peer(k), t,
            )
        slot = (lax.rem(y, 2), t)
        logs[k] = pltpu.make_async_remote_copy(
            src_ref=ls_out.at[k], dst_ref=ls_ref.at[slot], send_sem=l_send.at[k],
            recv_sem=l_recv.at[slot], device_id={"kv": row_peer(k), "tp": y // 2},
            device_id_type=MESH,
        )
        if k > 0:
            logs[k].start()
        else:
            @pl.when(jnp.logical_not(to_self))
            def _():
                logs[0].start()

            @pl.when(to_self)
            def _():
                ls_ref[slot] = ls_out[0]
    sent += [back[k] for k in range(1, NY)]

    loads[4].wait()
    halves[3].wait_recv()
    for k in (0, 1, 3, 2):
        if k > 0:
            back[k].wait_recv()
        ys = lax.rem(y + k, NY)
        weights = wo[ys // 2, pl.ds(pl.multiple_of(lax.rem(ys, 2) * 256, 256), 256), :]
        piece = att_out[0] if k == 0 else att_all[k]
        part = jnp.dot(piece, weights, preferred_element_type=F32)
        if k == 0:
            acc[...] = part
        elif k != 2:
            acc[...] += part
        else:
            projected = acc[...] + part
            square = jnp.mean(projected * projected, axis=-1, keepdims=True)
            out_ref[...] = (projected * lax.rsqrt(square + EPSILON)).astype(BF)

    for ys in range(2):
        for tt in range(2):
            @pl.when(jnp.logical_not((t * 2 + ys == y) & (t == tt)))
            def _():
                pltpu.make_async_remote_copy(
                    src_ref=ls_out.at[0], dst_ref=ls_ref.at[ys, tt], send_sem=l_send.at[0],
                    recv_sem=l_recv.at[ys, tt], device_id={"kv": kv, "tp": other},
                    device_id_type=MESH,
                ).wait_recv()
    for k in range(1, NY):
        logs[k].wait_send()

    @pl.when(jnp.logical_not(to_self))
    def _():
        logs[0].wait_send()

    for copy in sent + list(ups.values()) + list(downs.values()) + list(partner.values()):
        copy.wait_send()


def shards(tokens, w_query, w_key, w_value, w_out, chosen):
    rows, width = tokens.shape[1:]
    tables = rotary_tables(rows, 2 * NY * NZ)
    any_space = pl.BlockSpec(memory_space=pl.ANY)
    vmem = pl.BlockSpec(memory_space=pltpu.VMEM)
    dma = pltpu.SemaphoreType.DMA
    out, logs = pl.pallas_call(
        kernel,
        out_shape=(
            jax.ShapeDtypeStruct((rows, width), BF),
            jax.ShapeDtypeStruct((2, 2, 4, 4 * BLK), F32),
        ),
        in_specs=[vmem] * 4 + [any_space] * 5 + [vmem],
        out_specs=(vmem, vmem),
        scratch_shapes=[
            pltpu.VMEM((rows, width), BF),
            pltpu.VMEM((2,) + w_query.shape, BF),
            pltpu.VMEM((2,) + w_key.shape, BF),
            pltpu.VMEM((2,) + w_value.shape, BF),
            pltpu.VMEM((2,) + w_out.shape, BF),
            pltpu.VMEM((rows, 128), F32),
            pltpu.VMEM((rows, 128), F32),
            pltpu.VMEM((4, 4, BLK, 128), BF),
            pltpu.VMEM((NZ * NY * 8, BLK, 128), BF),
            pltpu.VMEM((NY, rows, 256), BF),
            pltpu.VMEM((NY, rows, 256), BF),
            pltpu.VMEM((NY, 8, PICK), jnp.int32),
            pltpu.SMEM((NY, 8, PICK), jnp.int32),
            pltpu.VMEM(((PICK + 1) * BLK, 128), BF),
            pltpu.VMEM((BLK, (PICK + 1) * BLK), BF),
            pltpu.VMEM(((PICK + 1) * BLK, 4 * BLK), F32),
            pltpu.VMEM(((PICK + 1) * BLK, 4 * BLK), BF),
            pltpu.VMEM((NY, rows, 256), BF),
            pltpu.VMEM((NY, rows, 256), BF),
            pltpu.VMEM((NY, 4, 4 * BLK), F32),
            pltpu.VMEM((rows, width), F32),
            dma((8,)), dma((4,)), dma((4,)), dma((4,)), dma((4,)),
            dma((4, 4)), dma((4, 4)), dma((4, 4)), dma((4, 4)),
            dma((NZ, 4)), dma((NZ, 4)), dma((4,)), dma((4,)), dma((4,)), dma((4,)),
            dma((4,)), dma((4,)), dma((4,)), dma((2, 2)),
        ],
        compiler_params=pltpu.CompilerParams(
            collective_id=0, has_side_effects=True, vmem_limit_bytes=48 * 1024 * 1024
        ),
    )(*tables, tokens[0], w_query, w_key, w_value, w_out, chosen[0])
    logs = logs.reshape(2, 2, 4, 4, BLK).transpose(1, 2, 4, 0, 3).reshape(2 * rows, 8)
    return out[None], logs[None]


def solution(mesh):
    placed = (
        P("dp", ("kv", "tp"), None),
        P(None, "tp"),
        P(None, "tp"),
        P(None, "tp"),
        P("tp", None),
        P("dp", "kv", None),
    )
    return jax.shard_map(
        shards,
        mesh=mesh,
        in_specs=placed,
        out_specs=(P("dp", ("kv", "tp"), None), P("dp", "kv", "tp")),
        check_vma=False,
    )
```

profile of v0, /device:TPU:1, one launch (start us, length us, event | category | flops | bytes accessed | tf_op | source)
XLA Modules:
  0.0 66.2 jit_solution(2713063407795208131)
XLA Ops:
  0.6 0.0 copy-start
  0.6 1.2 %copy-done = bf16[1024,512]{1,0:T(8,128)(2,1)S(1)} copy-done((bf16[1024,512]{1,0:T(8,128)(2,1)S(1)}, bf16[1024,512]{1,0:T(8,128)(2,1)}, u32[]{:S(2)}) %copy-start) | copy-done | bytes 1048600
  1.9 0.0 copy-start.1
  1.9 1.2 %copy-done.1 = bf16[512,1024]{1,0:T(8,128)(2,1)S(1)} copy-done((bf16[512,1024]{1,0:T(8,128)(2,1)S(1)}, bf16[512,1024]{1,0:T(8,128)(2,1)}, u32[]{:S(2)}) %copy-start.1) | copy-done | bytes 1048600
  3.1 0.0 copy-start.2
  3.1 1.0 %copy-done.2 = bf16[1,256,1024]{2,1,0:T(8,128)(2,1)S(1)} copy-done((bf16[1,256,1024]{2,1,0:T(8,128)(2,1)S(1)}, bf16[1,256,1024]{2,1,0:T(8,128)(2,1)}, u32[]{:S(2)}) %copy-start.2) | copy-done | bytes 524312
  4.1 0.0 copy-start.3
  4.1 0.9 %copy-done.3 = bf16[1024,128]{1,0:T(8,128)(2,1)S(1)} copy-done((bf16[1024,128]{1,0:T(8,128)(2,1)S(1)}, bf16[1024,128]{1,0:T(8,128)(2,1)}, u32[]{:S(2)}) %copy-start.3) | copy-done | bytes 262168
  5.1 0.0 copy-start.4
  5.1 0.9 %copy-done.4 = bf16[1024,128]{1,0:T(8,128)(2,1)S(1)} copy-done((bf16[1024,128]{1,0:T(8,128)(2,1)S(1)}, bf16[1024,128]{1,0:T(8,128)(2,1)}, u32[]{:S(2)}) %copy-start.4) | copy-done | bytes 262168
  6.0 0.0 copy-start.5
  6.0 0.9 %copy-done.5 = f32[256,128]{1,0:T(8,128)S(1)} copy-done((f32[256,128]{1,0:T(8,128)S(1)}, f32[256,128]{1,0:T(8,128)}, u32[]{:S(2)}) %copy-start.5) | copy-done | bytes 131096
  6.9 0.0 copy-start.6
  6.9 0.9 %copy-done.6 = f32[256,128]{1,0:T(8,128)S(1)} copy-done((f32[256,128]{1,0:T(8,128)S(1)}, f32[256,128]{1,0:T(8,128)}, u32[]{:S(2)}) %copy-start.6) | copy-done | bytes 131096
  7.8 0.0 copy-start.7
  7.8 0.8 %copy-done.7 = f32[64,128]{1,0:T(8,128)S(1)} copy-done((f32[64,128]{1,0:T(8,128)S(1)}, f32[64,128]{1,0:T(8,128)}, u32[]{:S(2)}) %copy-start.7) | copy-done | bytes 32792
  8.6 0.0 copy-start.8
  8.6 0.8 %copy-done.8 = f32[64,128]{1,0:T(8,128)S(1)} copy-done((f32[64,128]{1,0:T(8,128)S(1)}, f32[64,128]{1,0:T(8,128)}, u32[]{:S(2)}) %copy-start.8) | copy-done | bytes 32792
  9.4 0.0 copy-start.9
  9.4 0.7 %copy-done.9 = s32[1,8,15]{2,1,0:T(8,128)S(1)} copy-done((s32[1,8,15]{2,1,0:T(8,128)S(1)}, s32[1,8,15]{2,1,0:T(8,128)}, u32[]{:S(2)}) %copy-start.9) | copy-done | bytes 504
  10.0 54.6 %shard_map.113 = (bf16[256,1024]{1,0:T(8,128)(2,1)S(1)}, f32[2,2,4,256]{3,2,1,0:T(4,128)S(1)}) custom-call(f32[256,128]{1,0:T(8,128)S(1)} %copy-done.6, f32[256,128]{1,0:T(8,128)S(1)} %copy-done.5, f32[64,128]{1,0:T(8,128)S(1)} %copy-done.8, f32[64,128]{1,0:T(8,128)S(1)} %copy-done.7, bf16[256,1024]{1,0:T(8,128)(2,1)S(1)} %bitcast.7, ...), custom_call_target="tpu_custom_call" | custom-call | tf_op jit(solution)/shard_map/pallas_call | solution.py:344
  64.6 0.1 reshape.7
  64.7 0.7 %broadcast_in_dim_reshape.3 = f32[1,512,8]{1,2,0:T(8,128)} reshape(f32[2,4,64,2,4]{2,1,0,4,3:T(4,128)S(1)} %copy.12) | data formatting | bytes 32768 | tf_op jit(solution)/shard_map/broadcast_in_dim;reshape | solution.py:384
  65.4 0.8 %copy.14 = bf16[1,256,1024]{2,1,0:T(8,128)(2,1)} copy(bf16[1,256,1024]{2,1,0:T(8,128)(2,1)S(1)} %bitcast.6) | data formatting | bytes 1048576
  (1 shorter events, 0.0 us)
Async XLA Ops:
  0.6 1.2 %copy-start = (bf16[1024,512]{1,0:T(8,128)(2,1)S(1)}, bf16[1024,512]{1,0:T(8,128)(2,1)}, u32[]{:S(2)}) copy-start(bf16[1024,512]{1,0:T(8,128)(2,1)} %wq_hbm.1) | copy-start | bytes 3145732
  1.9 1.2 %copy-start.1 = (bf16[512,1024]{1,0:T(8,128)(2,1)S(1)}, bf16[512,1024]{1,0:T(8,128)(2,1)}, u32[]{:S(2)}) copy-start(bf16[512,1024]{1,0:T(8,128)(2,1)} %wo_hbm.1) | copy-start | bytes 3145732
  3.1 1.0 %copy-start.2 = (bf16[1,256,1024]{2,1,0:T(8,128)(2,1)S(1)}, bf16[1,256,1024]{2,1,0:T(8,128)(2,1)}, u32[]{:S(2)}) copy-start(bf16[1,256,1024]{2,1,0:T(8,128)(2,1)} %param.10) | copy-start | bytes 1572868
  4.1 0.9 %copy-start.3 = (bf16[1024,128]{1,0:T(8,128)(2,1)S(1)}, bf16[1024,128]{1,0:T(8,128)(2,1)}, u32[]{:S(2)}) copy-start(bf16[1024,128]{1,0:T(8,128)(2,1)} %wk_hbm.1) | copy-start | bytes 786436
  5.1 0.9 %copy-start.4 = (bf16[1024,128]{1,0:T(8,128)(2,1)S(1)}, bf16[1024,128]{1,0:T(8,128)(2,1)}, u32[]{:S(2)}) copy-start(bf16[1024,128]{1,0:T(8,128)(2,1)} %wv_hbm.1) | copy-start | bytes 786436
  6.0 0.9 %copy-start.5 = (f32[256,128]{1,0:T(8,128)S(1)}, f32[256,128]{1,0:T(8,128)}, u32[]{:S(2)}) copy-start(f32[256,128]{1,0:T(8,128)} %constant.9.clone.sr_ref) | copy-start | bytes 393220
  6.9 0.9 %copy-start.6 = (f32[256,128]{1,0:T(8,128)S(1)}, f32[256,128]{1,0:T(8,128)}, u32[]{:S(2)}) copy-start(f32[256,128]{1,0:T(8,128)} %constant.8.clone.cr_ref) | copy-start | bytes 393220
  7.8 0.8 %copy-start.7 = (f32[64,128]{1,0:T(8,128)S(1)}, f32[64,128]{1,0:T(8,128)}, u32[]{:S(2)}) copy-start(f32[64,128]{1,0:T(8,128)} %constant.11.clone.sb_ref) | copy-start | bytes 98308
  8.6 0.8 %copy-start.8 = (f32[64,128]{1,0:T(8,128)S(1)}, f32[64,128]{1,0:T(8,128)}, u32[]{:S(2)}) copy-start(f32[64,128]{1,0:T(8,128)} %constant.10.clone.cb_ref) | copy-start | bytes 98308
  9.4 0.7 %copy-start.9 = (s32[1,8,15]{2,1,0:T(8,128)S(1)}, s32[1,8,15]{2,1,0:T(8,128)}, u32[]{:S(2)}) copy-start(s32[1,8,15]{2,1,0:T(8,128)} %param.15) | copy-start | bytes 1444
where the time goes:
time: 66.7 us; the launch traced here: 66.2 us
  Pallas kernels  54.6 us (82%)
  local copies, waits for them, and re-layouts  11 us (16%)
  between operations  0.67 us (1%)
    pallas_call x1, Pallas kernels, shards(): pl.pallas_call(kernel, out_shape=(jax.ShapeDtypeStruct((rows, width), BF)...  54.6 us
    unnamed x21, local copies, waits for them, and re-layouts  10.2 us

commit v1 on v0

--- a/solution.py
+++ b/solution.py
@@ -36,9 +36,9 @@
 
 
 def kernel(
-    cr_ref, sr_ref, cb_ref, sb_ref, tok_hbm, wq_hbm, wk_hbm, wv_hbm, wo_hbm, chosen_ref,
+    cr_hbm, sr_hbm, cb_hbm, sb_hbm, tok_hbm, wq_hbm, wk_hbm, wv_hbm, wo_hbm, ch_hbm,
     out_ref, ls_ref,
-    tok, wq, wk, wv, wo, cosine, sine, kvs, kv_all, qs, q_all, ch_all, ch_smem,
+    cr_ref, sr_ref, cb_ref, sb_ref, tok, wq, wk, wv, wo, cosine, sine, kvs, kv_all, qs, q_all, ch_all, ch_smem,
     kg, vt, scores, probs, att_out, att_all, ls_out, acc,
     load_sem, w_send, w_recv, ky_send, ky_recv, up_send, up_recv, dn_send, dn_recv,
     pt_send, pt_recv, q_send, q_recv, c_send, c_recv, a_send, a_recv, l_send, l_recv,
@@ -69,7 +69,14 @@
         pltpu.make_async_copy(wq_hbm, wq.at[t], load_sem.at[3]),
         pltpu.make_async_copy(wo_hbm, wo.at[t], load_sem.at[4]),
     ]
-    for load in loads:
+    tables = [
+        pltpu.make_async_copy(a, b, load_sem.at[8 + i])
+        for i, (a, b) in enumerate(
+            ((cr_hbm, cr_ref), (sr_hbm, sr_ref), (cb_hbm, cb_ref), (sb_hbm, sb_ref))
+        )
+    ]
+    own_picks = pltpu.make_async_copy(ch_hbm, ch_all.at[0], load_sem.at[12])
+    for load in loads[:3] + tables + loads[3:] + [own_picks]:
         load.start()
 
     barrier = pltpu.get_barrier_semaphore()
@@ -93,9 +100,8 @@
     ]
     sent += halves
 
-    ch_all[0] = chosen_ref[...]
     picks = [
-        remote(chosen_ref, ch_all.at[NY - k], c_send.at[k], c_recv.at[NY - k], row_peer(k), t)
+        remote(ch_hbm, ch_all.at[NY - k], c_send.at[k], c_recv.at[NY - k], row_peer(k), t)
         for k in range(1, NY)
     ]
     sent += picks
@@ -105,6 +111,8 @@
     wide = lax.broadcasted_iota(jnp.int32, (4 * BLK, 128), 1)
     first = lax.rem(wide, HEAD_DIM) < HEAD_DIM // 2
 
+    for load in tables:
+        load.wait()
     base = kv * 2 + t
     cb, sb = cb_ref[pl.ds(base, 1), :], sb_ref[pl.ds(base, 1), :]
     cr, sr = cr_ref[...], sr_ref[...]
@@ -205,6 +213,7 @@
 
     for copy in picks:
         copy.wait_recv()
+    own_picks.wait()
     to_smem = pltpu.make_async_copy(ch_all, ch_smem, load_sem.at[7])
     to_smem.start()
     to_smem.wait()
@@ -347,9 +356,13 @@
             jax.ShapeDtypeStruct((rows, width), BF),
             jax.ShapeDtypeStruct((2, 2, 4, 4 * BLK), F32),
         ),
-        in_specs=[vmem] * 4 + [any_space] * 5 + [vmem],
+        in_specs=[any_space] * 10,
         out_specs=(vmem, vmem),
         scratch_shapes=[
+            pltpu.VMEM((rows, 128), F32),
+            pltpu.VMEM((rows, 128), F32),
+            pltpu.VMEM((2 * NY * NZ, 128), F32),
+            pltpu.VMEM((2 * NY * NZ, 128), F32),
             pltpu.VMEM((rows, width), BF),
             pltpu.VMEM((2,) + w_query.shape, BF),
             pltpu.VMEM((2,) + w_key.shape, BF),
@@ -371,13 +384,13 @@
             pltpu.VMEM((NY, rows, 256), BF),
             pltpu.VMEM((NY, 4, 4 * BLK), F32),
             pltpu.VMEM((rows, width), F32),
-            dma((8,)), dma((4,)), dma((4,)), dma((4,)), dma((4,)),
+            dma((13,)), dma((4,)), dma((4,)), dma((4,)), dma((4,)),
             dma((4, 4)), dma((4, 4)), dma((4, 4)), dma((4, 4)),
             dma((NZ, 4)), dma((NZ, 4)), dma((4,)), dma((4,)), dma((4,)), dma((4,)),
             dma((4,)), dma((4,)), dma((4,)), dma((2, 2)),
         ],
         compiler_params=pltpu.CompilerParams(
-            collective_id=0, has_side_effects=True, vmem_limit_bytes=48 * 1024 * 1024
+            collective_id=0, has_side_effects=True, vmem_limit_bytes=67_000_000
         ),
     )(*tables, tokens[0], w_query, w_key, w_value, w_out, chosen[0])
     logs = logs.reshape(2, 2, 4, 4, BLK).transpose(1, 2, 4, 0, 3).reshape(2 * rows, 8)

time: 66.7 us -> 59.8 us (0.90)
  local copies, waits for them, and re-layouts: 11 us -> 3.37 us
  Pallas kernels: 54.6 us -> 55.6 us
    unnamed x21 -> x1, local copies, waits for them, and re-layouts: 10.2 us -> 1.87 us
    pallas_call x1, Pallas kernels: 54.6 us -> 55.6 us  [shards(): pl.pallas_call(kernel, out_shape=(jax.ShapeDtypeStruct((rows, width), BF)...]
    reshape x1, local copies, waits for them, and re-layouts: 0.09 us -> 0.8 us  [shards(): logs.reshape(2, 2, 4, 4, BLK).transpose(1, 2, 4, 0, 3).reshape(2 * rows, 8)]
where the time goes in v1:
time: 59.8 us; the launch traced here: 59.6 us
  Pallas kernels  55.6 us (93%)
  local copies, waits for them, and re-layouts  3.37 us (6%)
  between operations  0.65 us (1%)
    pallas_call x1, Pallas kernels, shards(): pl.pallas_call(kernel, out_shape=(jax.ShapeDtypeStruct((rows, width), BF)...  55.6 us
    unnamed x1, local copies, waits for them, and re-layouts  1.87 us

profile of v1, /device:TPU:1, one launch (start us, length us, event | category | flops | bytes accessed | tf_op | source)
XLA Modules:
  0.0 59.6 jit_solution(4478316030604952106)
XLA Ops:
  0.6 55.6 %shard_map.113 = (bf16[256,1024]{1,0:T(8,128)(2,1)}, f32[2,2,4,256]{3,2,1,0:T(4,128)}) custom-call(f32[256,128]{1,0:T(8,128)} %constant.8.clone.cr_hbm, f32[256,128]{1,0:T(8,128)} %constant.9.clone.sr_hbm, f32[64,128]{1,0:T(8,128)} %constant.10.clone.cb_hbm, f32[64,128]{1,0:T(8,128)} %constant.11.clone.sb_hbm, bf16[256,1024]{1,0:T(8,128)(2,1)} %bitcast.7, ...), custom_call_target="tpu_custom_call" | custom-call | tf_op jit(solution)/shard_map/pallas_call | solution.py:353
  56.2 0.8 %reshape.7 = f32[2,2,4,4,64]{4,3,2,1,0:T(4,128)S(1)} reshape(f32[2,2,4,256]{3,2,1,0:T(4,128)} %get-tuple-element.5) | data formatting | bytes 32768 | tf_op jit(solution)/shard_map/reshape | solution.py:396
  57.0 0.7 %broadcast_in_dim_reshape.3 = f32[1,512,8]{1,2,0:T(8,128)} reshape(f32[2,4,64,2,4]{2,1,0,4,3:T(4,128)S(1)} %copy.12) | data formatting | bytes 32768 | tf_op jit(solution)/shard_map/broadcast_in_dim;reshape | solution.py:397
  57.7 1.9 %copy.14 = bf16[1,256,1024]{2,1,0:T(8,128)(2,1)} copy(bf16[1,256,1024]{2,1,0:T(8,128)(2,1)} %bitcast.6) | data formatting | bytes 1048576
  (1 shorter events, 0.0 us)

commit v2 on v1

v2 whole, which is shorter than its diff:
```python
import math

import jax
import jax.numpy as jnp
import numpy as np
from jax import lax
from jax.experimental import pallas as pl
from jax.experimental.pallas import tpu as pltpu
from jax.sharding import PartitionSpec as P

HEAD_DIM = 64
BLK = 64
PICK = 15
THETA_BASE = 10000.0
NEGATIVE = -1e30
EPSILON = 1e-06
MESH = pl.DeviceIdType.MESH
BF = jnp.bfloat16
F32 = jnp.float32
EXPONENT = math.log2(math.e) / math.sqrt(HEAD_DIM)
NY = 4
NZ = 8


def rotary_tables(rows, bases):
    half = HEAD_DIM // 2
    freq = THETA_BASE ** (-np.arange(half, dtype=np.float64) / half)
    freq = np.tile(freq, 128 // half)[None, :]
    offset = np.arange(rows, dtype=np.float64)[:, None] * freq
    base = np.arange(bases, dtype=np.float64)[:, None] * rows * freq
    return [
        np.asarray(a, np.float32)
        for a in (np.cos(offset), np.sin(offset), np.cos(base), np.sin(base))
    ]


def kernel(
    cr_hbm, sr_hbm, cb_hbm, sb_hbm, tok_hbm, wq_hbm, wk_hbm, wv_hbm, wo_hbm, ch_hbm,
    out_ref, ls_ref,
    cr_ref, sr_ref, cb_ref, sb_ref, tok, wq, wk, wv, wo, cosine, sine, k_own, v_own,
    k_all, v_all, qs, q_all, ch_all, ch_smem, kg, vt, scores, probs, inverse,
    att_out, att_all, ls_out, acc,
    load_sem, w_send, w_recv, ky_send, ky_recv, vy_send, vy_recv,
    k_up_send, k_up_recv, k_dn_send, k_dn_recv, k_pt_send, k_pt_recv,
    v_up_send, v_up_recv, v_dn_send, v_dn_recv, v_pt_send, v_pt_recv,
    q_send, q_recv, c_send, c_recv, a_send, a_recv, l_send, l_recv,
):
    kv = lax.axis_index("kv")
    t = lax.axis_index("tp")
    z, y = kv // NY, kv % NY
    other = 1 - t

    def row_chip(k):
        return lax.rem(y + k, NY)

    def row_peer(k):
        return z * NY + row_chip(k)

    def chunk(zz, yy):
        return pl.ds(((zz * NY + yy) * 2 + t) * 4, 4)

    def remote(src, dst, send, recv, kv_to, tp_to):
        return pltpu.make_async_remote_copy(
            src_ref=src, dst_ref=dst, send_sem=send, recv_sem=recv,
            device_id={"kv": kv_to, "tp": tp_to}, device_id_type=MESH,
        )

    loads = [
        pltpu.make_async_copy(tok_hbm, tok, load_sem.at[0]),
        pltpu.make_async_copy(wk_hbm, wk.at[t], load_sem.at[1]),
        pltpu.make_async_copy(wv_hbm, wv.at[t], load_sem.at[2]),
        pltpu.make_async_copy(wq_hbm, wq.at[t], load_sem.at[3]),
        pltpu.make_async_copy(wo_hbm, wo.at[t], load_sem.at[4]),
    ]
    tables = [
        pltpu.make_async_copy(a, b, load_sem.at[8 + i])
        for i, (a, b) in enumerate(
            ((cr_hbm, cr_ref), (sr_hbm, sr_ref), (cb_hbm, cb_ref), (sb_hbm, sb_ref))
        )
    ]
    own_picks = pltpu.make_async_copy(ch_hbm, ch_all.at[0], load_sem.at[12])
    for load in loads[:3] + tables + loads[3:] + [own_picks]:
        load.start()

    barrier = pltpu.get_barrier_semaphore()
    peers = [(row_peer(k), tt) for k in range(1, NY) for tt in (t, other)]
    peers += [(kv, other)]
    z_up = lax.rem(z + 1, NZ) * NY + y
    z_dn = lax.rem(z + NZ - 1, NZ) * NY + y
    peers += [(z_up, t), (z_dn, t)]
    for kv_to, tp_to in peers:
        pl.semaphore_signal(
            barrier, inc=1, device_id={"kv": kv_to, "tp": tp_to}, device_id_type=MESH
        )

    left = lax.broadcasted_iota(jnp.int32, (BLK, 128), 1) < BLK
    left_half = lax.broadcasted_iota(jnp.int32, (BLK // 2, 128), 1) < BLK
    wide = lax.broadcasted_iota(jnp.int32, (4 * BLK, 128), 1)
    first = lax.rem(wide, HEAD_DIM) < HEAD_DIM // 2

    for load in tables:
        load.wait()
    base = kv * 2 + t
    cb, sb = cb_ref[pl.ds(base, 1), :], sb_ref[pl.ds(base, 1), :]
    cr, sr = cr_ref[...], sr_ref[...]
    cosine[...] = cb * cr - sb * sr
    turned = sb * cr + cb * sr
    sine[...] = jnp.where(first, -turned, turned)

    def rotate(x):
        swapped = jnp.where(first, pltpu.roll(x, 96, 1), pltpu.roll(x, 32, 1))
        return x * cosine[...] + swapped * sine[...]

    def project_kv(half):
        tokens = tok[...]
        keys = jnp.dot(tokens, wk[half], preferred_element_type=F32).astype(BF).astype(F32)
        keys = rotate(keys)
        keys = (keys, pltpu.roll(keys, 64, 1))
        values = jnp.dot(tokens, wv[half], preferred_element_type=F32).T
        values = [values[:, i * 128 : i * 128 + 128] for i in range(2)]
        values = [(x, pltpu.roll(x, 64, 1)) for x in values]
        for e in range(2):
            for j in range(4):
                low = keys[e][j * 64 : j * 64 + 32]
                high = keys[1 - e][j * 64 + 32 : j * 64 + 64]
                k_own[2 * half + e, j] = jnp.where(left_half, low, high).astype(BF)
                pair = values[j // 2]
                low = pair[j % 2][e * 64 : e * 64 + 32]
                high = pair[1 - j % 2][e * 64 + 32 : e * 64 + 64]
                v_own[2 * half + e, j] = jnp.where(left_half, low, high).astype(BF)

    def project_q(half):
        tokens = tok[...]
        full = jnp.dot(tokens, wq[half], preferred_element_type=F32)
        for n in range(4):
            x = full[:, n * 128 : n * 128 + 128].astype(BF).astype(F32)
            qs[2 * half + n // 2, :, (n % 2) * 128 : (n % 2) * 128 + 128] = rotate(x).astype(BF)

    for load in loads[:3]:
        load.wait()
    project_kv(t)

    pl.semaphore_wait(barrier, len(peers))

    halves = [
        remote(wk_hbm, wk.at[t], w_send.at[0], w_recv.at[0], kv, other),
        remote(wv_hbm, wv.at[t], w_send.at[1], w_recv.at[1], kv, other),
        remote(wq_hbm, wq.at[t], w_send.at[2], w_recv.at[2], kv, other),
        remote(wo_hbm, wo.at[t], w_send.at[3], w_recv.at[3], kv, other),
    ]

    def to_owner(own, every, send, recv, head):
        return remote(
            own.at[head], every.at[chunk(z, y)], send.at[head], recv.at[y], z * NY + head, t
        )

    def key_to_owner(head):
        return to_owner(k_own, k_all, ky_send, ky_recv, head)

    def value_to_owner(head):
        return to_owner(v_own, v_all, vy_send, vy_recv, head)

    def send_heads(half):
        for make in (key_to_owner, value_to_owner):
            for e in range(2):
                head = 2 * half + e

                @pl.when(head != y)
                def _():
                    make(head).start()

    for copy in halves[:2]:
        copy.start()
    send_heads(t)
    picks = [
        remote(ch_hbm, ch_all.at[NY - k], c_send.at[k], c_recv.at[NY - k], row_peer(k), t)
        for k in range(1, NY)
    ]
    for copy in halves[2:] + picks:
        copy.start()

    loads[3].wait()
    project_q(t)
    for copy in halves[:2]:
        copy.wait_recv()
    project_kv(other)
    send_heads(other)

    def ring(every, up_send, up_recv, dn_send, dn_recv, pt_send, pt_recv):
        def place(zz, k):
            return every.at[chunk(zz, row_chip(k))]

        def up(s, k, src=None):
            spot = place(lax.rem(z + NZ - s, NZ), k)
            src = spot if src is None else src
            return remote(src, spot, up_send.at[s, k], up_recv.at[s, k], z_up, t)

        def down(s, k, src=None):
            spot = place(lax.rem(z + s, NZ), k)
            src = spot if src is None else src
            return remote(src, spot, dn_send.at[s, k], dn_recv.at[s, k], z_dn, t)

        def partner(rel, k, src=None):
            spot = place(lax.rem(z + rel, NZ), k)
            src = spot if src is None else src
            return remote(src, spot, pt_send.at[rel, k], pt_recv.at[rel, k], kv, other)

        return up, down, partner

    k_ring = ring(k_all, k_up_send, k_up_recv, k_dn_send, k_dn_recv, k_pt_send, k_pt_recv)
    v_ring = ring(v_all, v_up_send, v_up_recv, v_dn_send, v_dn_recv, v_pt_send, v_pt_recv)

    def begin(group, k, src=None):
        up, down, partner = group
        up(0, k, src).start()
        down(0, k, src).start()
        partner(0, k, src).start()

    def step(group, s, k):
        up, down, partner = group
        if s < NZ // 2:
            turn = s == NZ // 2 - 1
            up(s - 1, k).wait_recv()
            if not turn:
                up(s, k).start()
            else:
                pl.when(k < 2)(lambda: up(s, k).start())
            partner(NZ - s, k).start()
            down(s - 1, k).wait_recv()
            if not turn:
                down(s, k).start()
            else:
                pl.when(k >= 2)(lambda: down(s, k).start())
            partner(s, k).start()
        else:
            pl.when(k < 2)(lambda: up(s - 1, k).wait_recv())
            pl.when(k >= 2)(lambda: down(s - 1, k).wait_recv())
            partner(s, k).start()

    mine = [
        pltpu.make_async_copy(k_own.at[y], k_all.at[chunk(z, y)], load_sem.at[5]),
        pltpu.make_async_copy(v_own.at[y], v_all.at[chunk(z, y)], load_sem.at[7]),
    ]
    begin(k_ring, 0, k_own.at[y])
    for copy in mine:
        copy.start()

    halves[2].wait_recv()
    project_q(other)
    own_q = pltpu.make_async_copy(qs.at[y], q_all.at[0], load_sem.at[6])
    own_q.start()
    queries = [None] * NY
    for k in (2, 1, 3):
        queries[NY - k] = remote(
            qs.at[row_chip(k)], q_all.at[NY - k], q_send.at[k], q_recv.at[NY - k],
            row_peer(k), t,
        )
        queries[NY - k].start()

    def from_row(every, own, send, recv, k):
        remote(
            own.at[0], every.at[chunk(z, row_chip(k))], send.at[0], recv.at[row_chip(k)],
            row_peer(k), t,
        ).wait_recv()

    for k in (1, 3, 2):
        from_row(k_all, k_own, ky_send, ky_recv, k)
        begin(k_ring, k)
    for s in range(1, NZ // 2):
        for k in range(NY):
            step(k_ring, s, k)
    for copy in mine:
        copy.wait()
    begin(v_ring, 0)
    for k in (1, 2, 3):
        from_row(v_all, v_own, vy_send, vy_recv, k)
        begin(v_ring, k)
    for k in range(NY):
        step(k_ring, NZ // 2, k)

    for copy in picks:
        copy.wait_recv()
    own_picks.wait()
    to_smem = pltpu.make_async_copy(ch_all, ch_smem, load_sem.at[13])
    to_smem.start()
    to_smem.wait()
    own_q.wait()
    for k in range(1, NY):
        queries[k].wait_recv()
    for rel in range(NZ):
        for k in range(NY):
            k_ring[2](rel, k).wait_recv()

    key_pos = lax.broadcasted_iota(jnp.int32, (BLK, 4 * BLK), 0)
    query_pos = lax.rem(lax.broadcasted_iota(jnp.int32, (BLK, 4 * BLK), 1), BLK)
    causal = key_pos <= query_pos
    half_blk = BLK // 2

    def own_block(k, jb):
        return (z * NY + row_chip(k)) * 8 + t * 4 + jb

    def weigh(k, jb):
        rows = pl.ds(pl.multiple_of(jb * BLK, BLK), BLK)
        heads = []
        for n in range(2):
            x = q_all[k, rows, n * 128 : n * 128 + 128].astype(F32)
            swapped = pltpu.roll(x, 64, 1)
            heads += [jnp.where(left, x, swapped), jnp.where(left, swapped, x)]
        q2 = jnp.concatenate(heads, axis=0).astype(BF)
        bias = []
        for j in range(PICK + 1):
            if j < PICK:
                pick = ch_smem[k, t * 4 + jb, j]
                bias.append(jnp.where(pick < 0, NEGATIVE, 0.0).astype(F32))
                block = k_all[jnp.maximum(pick, 0)]
            else:
                block = k_all[own_block(k, jb)]
            nothing = jnp.zeros_like(block)
            kg[j * BLK : j * BLK + half_blk, :] = jnp.where(left_half, block, nothing)
            kg[j * BLK + half_blk : j * BLK + BLK, :] = jnp.where(left_half, nothing, block)
        scores[...] = lax.dot_general(
            kg[...], q2, (((1,), (1,)), ((), ())), preferred_element_type=F32
        )
        tail = jnp.where(causal, scores[PICK * BLK :, :], NEGATIVE)
        top = jnp.max(tail, axis=0, keepdims=True)
        for j in range(PICK):
            here = jnp.max(scores[j * BLK : j * BLK + BLK, :], axis=0, keepdims=True)
            top = jnp.maximum(top, here + bias[j])
        total = jnp.zeros((1, 4 * BLK), F32)
        for j in range(PICK + 1):
            s = tail if j == PICK else scores[j * BLK : j * BLK + BLK, :]
            shift = top if j == PICK else top - bias[j]
            p = jnp.exp2((s - shift) * EXPONENT)
            total = total + jnp.sum(p, axis=0, keepdims=True)
            probs[k * 4 + jb, j * BLK : j * BLK + BLK, :] = p.astype(BF)
        inverse[k, pl.ds(jb, 1), :] = 1.0 / total
        ls_out[k, pl.ds(jb, 1), :] = top * HEAD_DIM**-0.5 + jnp.log(total)

    def combine(k, jb):
        rows = pl.ds(pl.multiple_of(jb * BLK, BLK), BLK)
        previous = None
        for j in range(PICK + 1):
            if j < PICK:
                block = v_all[jnp.maximum(ch_smem[k, t * 4 + jb, j], 0)]
            else:
                block = v_all[own_block(k, jb)]
            block = block.astype(F32)
            if j % 2 == 1:
                low = jnp.where(left_half, previous, pltpu.roll(block, 64, 1))
                high = jnp.where(left_half, pltpu.roll(previous, 64, 1), block)
                columns = slice((j // 2) * 128, (j // 2) * 128 + 128)
                vt[:half_blk, columns] = low.astype(BF)
                vt[half_blk:, columns] = high.astype(BF)
            previous = block
        mixed = jnp.dot(vt[...], probs[k * 4 + jb], preferred_element_type=F32)
        turned_back = (mixed * inverse[k, pl.ds(jb, 1), :]).T
        parts = [turned_back[h * BLK : h * BLK + BLK] for h in range(4)]
        att_out[k, rows, :] = jnp.concatenate(parts, axis=1).astype(BF)

    to_self = y // 2 == t
    slot = (lax.rem(y, 2), t)

    def log_piece(k):
        return remote(
            ls_out.at[k], ls_ref.at[slot], l_send.at[k], l_recv.at[slot], row_peer(k), y // 2
        )

    for s, k in enumerate((2, 1, 3, 0)):
        @pl.loop(0, 4)
        def _(jb):
            weigh(k, jb)
            step(v_ring, s + 1, jb)

        if k > 0:
            log_piece(k).start()
        else:
            pl.when(jnp.logical_not(to_self))(lambda: log_piece(0).start())

            @pl.when(to_self)
            def _():
                ls_ref[slot] = ls_out[0]

    for rel in range(NZ):
        for k in range(NY):
            v_ring[2](rel, k).wait_recv()

    back = {}
    for k in (2, 1, 3, 0):
        @pl.loop(0, 4)
        def _(jb):
            combine(k, jb)

        if k > 0:
            back[NY - k] = remote(
                att_out.at[k], att_all.at[NY - k], a_send.at[k], a_recv.at[NY - k],
                row_peer(k), t,
            )
            back[NY - k].start()

    loads[4].wait()
    halves[3].wait_recv()
    for k in (0, 1, 3, 2):
        if k > 0:
            back[k].wait_recv()
        ys = row_chip(k)
        weights = wo[ys // 2, pl.ds(pl.multiple_of(lax.rem(ys, 2) * 256, 256), 256), :]
        piece = att_out[0] if k == 0 else att_all[k]
        part = jnp.dot(piece, weights, preferred_element_type=F32)
        if k == 0:
            acc[...] = part
        elif k != 2:
            acc[...] += part
        else:
            projected = acc[...] + part
            square = jnp.mean(projected * projected, axis=-1, keepdims=True)
            out_ref[...] = (projected * lax.rsqrt(square + EPSILON)).astype(BF)

    for ys in range(2):
        for tt in range(2):
            @pl.when(jnp.logical_not((t * 2 + ys == y) & (t == tt)))
            def _():
                remote(
                    ls_out.at[0], ls_ref.at[ys, tt], l_send.at[0], l_recv.at[ys, tt], kv, other
                ).wait_recv()
    for k in range(1, NY):
        log_piece(k).wait_send()
    pl.when(jnp.logical_not(to_self))(lambda: log_piece(0).wait_send())
    for k in range(1, NY):
        key_to_owner(row_chip(k)).wait_send()
        value_to_owner(row_chip(k)).wait_send()
        queries[k].wait_send()
        back[k].wait_send()
    for copy in halves + picks:
        copy.wait_send()
    for up, down, partner in (k_ring, v_ring):
        for k in range(NY):
            for s in range(NZ // 2):
                if s < NZ // 2 - 1 or k < 2:
                    up(s, k).wait_send()
                if s < NZ // 2 - 1 or k >= 2:
                    down(s, k).wait_send()
            for rel in range(NZ):
                partner(rel, k).wait_send()


def shards(tokens, w_query, w_key, w_value, w_out, chosen):
    rows, width = tokens.shape[1:]
    tables = rotary_tables(rows, 2 * NY * NZ)
    any_space = pl.BlockSpec(memory_space=pl.ANY)
    vmem = pl.BlockSpec(memory_space=pltpu.VMEM)
    dma = pltpu.SemaphoreType.DMA
    out, logs = pl.pallas_call(
        kernel,
        out_shape=(
            jax.ShapeDtypeStruct((rows, width), BF),
            jax.ShapeDtypeStruct((2, 2, 4, 4 * BLK), F32),
        ),
        in_specs=[any_space] * 10,
        out_specs=(vmem, vmem),
        scratch_shapes=[
            pltpu.VMEM((rows, 128), F32),
            pltpu.VMEM((rows, 128), F32),
            pltpu.VMEM((2 * NY * NZ, 128), F32),
            pltpu.VMEM((2 * NY * NZ, 128), F32),
            pltpu.VMEM((rows, width), BF),
            pltpu.VMEM((2,) + w_query.shape, BF),
            pltpu.VMEM((2,) + w_key.shape, BF),
            pltpu.VMEM((2,) + w_value.shape, BF),
            pltpu.VMEM((2,) + w_out.shape, BF),
            pltpu.VMEM((rows, 128), F32),
            pltpu.VMEM((rows, 128), F32),
            pltpu.VMEM((4, 4, BLK // 2, 128), BF),
            pltpu.VMEM((4, 4, BLK // 2, 128), BF),
            pltpu.VMEM((NZ * NY * 8, BLK // 2, 128), BF),
            pltpu.VMEM((NZ * NY * 8, BLK // 2, 128), BF),
            pltpu.VMEM((NY, rows, 256), BF),
            pltpu.VMEM((NY, rows, 256), BF),
            pltpu.VMEM((NY, 8, PICK), jnp.int32),
            pltpu.SMEM((NY, 8, PICK), jnp.int32),
            pltpu.VMEM(((PICK + 1) * BLK, 128), BF),
            pltpu.VMEM((BLK, (PICK + 1) * BLK), BF),
            pltpu.VMEM(((PICK + 1) * BLK, 4 * BLK), F32),
            pltpu.VMEM((NY * 4, (PICK + 1) * BLK, 4 * BLK), BF),
            pltpu.VMEM((NY, 4, 4 * BLK), F32),
            pltpu.VMEM((NY, rows, 256), BF),
            pltpu.VMEM((NY, rows, 256), BF),
            pltpu.VMEM((NY, 4, 4 * BLK), F32),
            pltpu.VMEM((rows, width), F32),
            dma((14,)), dma((4,)), dma((4,)), dma((4,)), dma((4,)), dma((4,)), dma((4,)),
            dma((4, 4)), dma((4, 4)), dma((4, 4)), dma((4, 4)), dma((NZ, 4)), dma((NZ, 4)),
            dma((4, 4)), dma((4, 4)), dma((4, 4)), dma((4, 4)), dma((NZ, 4)), dma((NZ, 4)),
            dma((4,)), dma((4,)), dma((4,)), dma((4,)),
            dma((4,)), dma((4,)), dma((4,)), dma((2, 2)),
        ],
        compiler_params=pltpu.CompilerParams(
            collective_id=0, has_side_effects=True, vmem_limit_bytes=67_000_000
        ),
    )(*tables, tokens[0], w_query, w_key, w_value, w_out, chosen[0])
    logs = logs.reshape(2, 2, 4, 4, BLK).transpose(1, 2, 4, 0, 3).reshape(2 * rows, 8)
    return out[None], logs[None]


def solution(mesh):
    placed = (
        P("dp", ("kv", "tp"), None),
        P(None, "tp"),
        P(None, "tp"),
        P(None, "tp"),
        P("tp", None),
        P("dp", "kv", None),
    )
    return jax.shard_map(
        shards,
        mesh=mesh,
        in_specs=placed,
        out_specs=(P("dp", ("kv", "tp"), None), P("dp", "kv", "tp")),
        check_vma=False,
    )
```

time: 59.8 us -> 63.7 us (1.065)
  Pallas kernels: 55.6 us -> 59.5 us
    pallas_call x1, Pallas kernels: 55.6 us -> 59.5 us  [shards(): pl.pallas_call(kernel, out_shape=(jax.ShapeDtypeStruct((rows, width), BF)...]
where the time goes in v2:
time: 63.7 us; the launch traced here: 63.5 us
  Pallas kernels  59.5 us (93%)
  local copies, waits for them, and re-layouts  3.37 us (5%)
  between operations  0.65 us (1%)
    pallas_call x1, Pallas kernels, shards(): pl.pallas_call(kernel, out_shape=(jax.ShapeDtypeStruct((rows, width), BF)...  59.5 us
    unnamed x1, local copies, waits for them, and re-layouts  1.87 us

profile of v2, /device:TPU:1, one launch (start us, length us, event | category | flops | bytes accessed | tf_op | source)
XLA Modules:
  0.0 63.5 jit_solution(18008994994058840505)
XLA Ops:
  0.6 59.5 %shard_map.113 = (bf16[256,1024]{1,0:T(8,128)(2,1)}, f32[2,2,4,256]{3,2,1,0:T(4,128)}) custom-call(f32[256,128]{1,0:T(8,128)} %constant.8.clone.cr_hbm, f32[256,128]{1,0:T(8,128)} %constant.9.clone.sr_hbm, f32[64,128]{1,0:T(8,128)} %constant.10.clone.cb_hbm, f32[64,128]{1,0:T(8,128)} %constant.11.clone.sb_hbm, bf16[256,1024]{1,0:T(8,128)(2,1)} %bitcast.7, ...), custom_call_target="tpu_custom_call" | custom-call | tf_op jit(solution)/shard_map/pallas_call | solution.py:452
  60.1 0.8 %reshape.7 = f32[2,2,4,4,64]{4,3,2,1,0:T(4,128)S(1)} reshape(f32[2,2,4,256]{3,2,1,0:T(4,128)} %get-tuple-element.5) | data formatting | bytes 32768 | tf_op jit(solution)/shard_map/reshape | solution.py:499
  61.0 0.7 %broadcast_in_dim_reshape.3 = f32[1,512,8]{1,2,0:T(8,128)} reshape(f32[2,4,64,2,4]{2,1,0,4,3:T(4,128)S(1)} %copy.12) | data formatting | bytes 32768 | tf_op jit(solution)/shard_map/broadcast_in_dim;reshape | solution.py:500
  61.7 1.9 %copy.14 = bf16[1,256,1024]{2,1,0:T(8,128)(2,1)} copy(bf16[1,256,1024]{2,1,0:T(8,128)(2,1)} %bitcast.6) | data formatting | bytes 1048576
  (1 shorter events, 0.0 us)

commit v3 on v2

--- a/solution.py
+++ b/solution.py
@@ -41,8 +41,8 @@
     k_all, v_all, qs, q_all, ch_all, ch_smem, kg, vt, scores, probs, inverse,
     att_out, att_all, ls_out, acc,
     load_sem, w_send, w_recv, ky_send, ky_recv, vy_send, vy_recv,
-    k_up_send, k_up_recv, k_dn_send, k_dn_recv, k_pt_send, k_pt_recv,
-    v_up_send, v_up_recv, v_dn_send, v_dn_recv, v_pt_send, v_pt_recv,
+    k_own_send, k_own_recv, k_up_send, k_up_recv, k_dn_send, k_dn_recv, k_pt_send, k_pt_recv,
+    v_own_send, v_own_recv, v_up_send, v_up_recv, v_dn_send, v_dn_recv, v_pt_send, v_pt_recv,
     q_send, q_recv, c_send, c_recv, a_send, a_recv, l_send, l_recv,
 ):
     kv = lax.axis_index("kv")
@@ -57,7 +57,17 @@
         return z * NY + row_chip(k)
 
     def chunk(zz, yy):
-        return pl.ds(((zz * NY + yy) * 2 + t) * 4, 4)
+        return pl.ds(zz * 32 + t * 16 + yy * 4, 4)
+
+    def near(r):
+        c, i = r // 2, r % 2
+        return 2 * lax.rem(y // 2 + c, 2) + lax.rem(y * (1 - c) + i, 2)
+
+    def pair_chunk(zz, c):
+        return pl.ds(zz * 32 + t * 16 + lax.rem(y // 2 + c, 2) * 8, 8)
+
+    def place_of(block):
+        return block // 32 * 32 + block // 4 % 2 * 16 + block // 8 % 4 * 4 + block % 4
 
     def remote(src, dst, send, recv, kv_to, tp_to):
         return pltpu.make_async_remote_copy(
@@ -186,56 +196,67 @@
     project_kv(other)
     send_heads(other)
 
-    def ring(every, up_send, up_recv, dn_send, dn_recv, pt_send, pt_recv):
-        def place(zz, k):
-            return every.at[chunk(zz, row_chip(k))]
-
-        def up(s, k, src=None):
-            spot = place(lax.rem(z + NZ - s, NZ), k)
-            src = spot if src is None else src
-            return remote(src, spot, up_send.at[s, k], up_recv.at[s, k], z_up, t)
-
-        def down(s, k, src=None):
-            spot = place(lax.rem(z + s, NZ), k)
-            src = spot if src is None else src
-            return remote(src, spot, dn_send.at[s, k], dn_recv.at[s, k], z_dn, t)
-
-        def partner(rel, k, src=None):
-            spot = place(lax.rem(z + rel, NZ), k)
-            src = spot if src is None else src
-            return remote(src, spot, pt_send.at[rel, k], pt_recv.at[rel, k], kv, other)
+    def ring(every, own_send, own_recv, up_send, up_recv, dn_send, dn_recv, pt_send, pt_recv):
+        def up(s, c, src=None):
+            if s == 0:
+                spot = every.at[chunk(z, near(c))]
+                return remote(
+                    spot if src is None else src, spot, own_send.at[0, c], own_recv.at[0, c],
+                    z_up, t,
+                )
+            spot = every.at[pair_chunk(lax.rem(z + NZ - s, NZ), c)]
+            return remote(spot, spot, up_send.at[s, c], up_recv.at[s, c], z_up, t)
+
+        def down(s, c, src=None):
+            if s == 0:
+                spot = every.at[chunk(z, near(c))]
+                return remote(
+                    spot if src is None else src, spot, own_send.at[1, c], own_recv.at[1, c],
+                    z_dn, t,
+                )
+            spot = every.at[pair_chunk(lax.rem(z + s, NZ), c)]
+            return remote(spot, spot, dn_send.at[s, c], dn_recv.at[s, c], z_dn, t)
+
+        def partner(rel, c):
+            spot = every.at[pair_chunk(lax.rem(z + rel, NZ), c)]
+            return remote(spot, spot, pt_send.at[rel, c], pt_recv.at[rel, c], kv, other)
 
         return up, down, partner
 
-    k_ring = ring(k_all, k_up_send, k_up_recv, k_dn_send, k_dn_recv, k_pt_send, k_pt_recv)
-    v_ring = ring(v_all, v_up_send, v_up_recv, v_dn_send, v_dn_recv, v_pt_send, v_pt_recv)
-
-    def begin(group, k, src=None):
+    k_ring = ring(
+        k_all, k_own_send, k_own_recv, k_up_send, k_up_recv, k_dn_send, k_dn_recv,
+        k_pt_send, k_pt_recv,
+    )
+    v_ring = ring(
+        v_all, v_own_send, v_own_recv, v_up_send, v_up_recv, v_dn_send, v_dn_recv,
+        v_pt_send, v_pt_recv,
+    )
+
+    def begin(group, r, src=None):
+        group[0](0, r, src).start()
+        group[1](0, r, src).start()
+
+    def step(group, s, c):
         up, down, partner = group
-        up(0, k, src).start()
-        down(0, k, src).start()
-        partner(0, k, src).start()
-
-    def step(group, s, k):
-        up, down, partner = group
-        if s < NZ // 2:
+        if s == 1:
+            for both in (up, down):
+                for i in range(2):
+                    both(0, 2 * c + i).wait_recv()
+                both(1, c).start()
+            partner(NZ - 1, c).start()
+            partner(1, c).start()
+        elif s < NZ // 2:
             turn = s == NZ // 2 - 1
-            up(s - 1, k).wait_recv()
-            if not turn:
-                up(s, k).start()
-            else:
-                pl.when(k < 2)(lambda: up(s, k).start())
-            partner(NZ - s, k).start()
-            down(s - 1, k).wait_recv()
-            if not turn:
-                down(s, k).start()
-            else:
-                pl.when(k >= 2)(lambda: down(s, k).start())
-            partner(s, k).start()
+            up(s - 1, c).wait_recv()
+            pl.when(not turn or c == 0)(lambda: up(s, c).start())
+            partner(NZ - s, c).start()
+            down(s - 1, c).wait_recv()
+            pl.when(not turn or c == 1)(lambda: down(s, c).start())
+            partner(s, c).start()
         else:
-            pl.when(k < 2)(lambda: up(s - 1, k).wait_recv())
-            pl.when(k >= 2)(lambda: down(s - 1, k).wait_recv())
-            partner(s, k).start()
+            pl.when(c == 0)(lambda: up(s - 1, c).wait_recv())
+            pl.when(c == 1)(lambda: down(s - 1, c).wait_recv())
+            partner(s, c).start()
 
     mine = [
         pltpu.make_async_copy(k_own.at[y], k_all.at[chunk(z, y)], load_sem.at[5]),
@@ -257,49 +278,69 @@
         )
         queries[NY - k].start()
 
-    def from_row(every, own, send, recv, k):
-        remote(
-            own.at[0], every.at[chunk(z, row_chip(k))], send.at[0], recv.at[row_chip(k)],
-            row_peer(k), t,
-        ).wait_recv()
-
-    for k in (1, 3, 2):
-        from_row(k_all, k_own, ky_send, ky_recv, k)
-        begin(k_ring, k)
-    for s in range(1, NZ // 2):
-        for k in range(NY):
-            step(k_ring, s, k)
-    for copy in mine:
-        copy.wait()
-    begin(v_ring, 0)
-    for k in (1, 2, 3):
-        from_row(v_all, v_own, vy_send, vy_recv, k)
-        begin(v_ring, k)
-    for k in range(NY):
-        step(k_ring, NZ // 2, k)
-
     for copy in picks:
         copy.wait_recv()
     own_picks.wait()
     to_smem = pltpu.make_async_copy(ch_all, ch_smem, load_sem.at[13])
     to_smem.start()
+
+    def from_row(every, own, send, recv, r):
+        from_y = near(r)
+        remote(
+            own.at[0], every.at[chunk(z, from_y)], send.at[0], recv.at[from_y],
+            z * NY + from_y, t,
+        ).wait_recv()
+
+    for r in (1, 2, 3):
+        from_row(k_all, k_own, ky_send, ky_recv, r)
+        begin(k_ring, r)
+    for copy in mine:
+        copy.wait()
+    for c in range(2):
+        k_ring[2](0, c).start()
+    for s in range(1, NZ // 2):
+        for c in range(2):
+            step(k_ring, s, c)
+    begin(v_ring, 0)
+    for r in (1, 2, 3):
+        from_row(v_all, v_own, vy_send, vy_recv, r)
+        begin(v_ring, r)
+    for c in range(2):
+        v_ring[2](0, c).start()
+    for c in range(2):
+        step(k_ring, NZ // 2, c)
+
     to_smem.wait()
     own_q.wait()
     for k in range(1, NY):
         queries[k].wait_recv()
     for rel in range(NZ):
-        for k in range(NY):
-            k_ring[2](rel, k).wait_recv()
+        for c in range(2):
+            k_ring[2](rel, c).wait_recv()
 
     key_pos = lax.broadcasted_iota(jnp.int32, (BLK, 4 * BLK), 0)
     query_pos = lax.rem(lax.broadcasted_iota(jnp.int32, (BLK, 4 * BLK), 1), BLK)
     causal = key_pos <= query_pos
     half_blk = BLK // 2
 
-    def own_block(k, jb):
-        return (z * NY + row_chip(k)) * 8 + t * 4 + jb
-
-    def weigh(k, jb):
+    def own_place(k, jb):
+        return z * 32 + t * 16 + row_chip(k) * 4 + jb
+
+    def gather_keys(k, jb, u):
+        bias = []
+        for j in range(PICK + 1):
+            if j < PICK:
+                pick = ch_smem[k, t * 4 + jb, j]
+                bias.append(jnp.where(pick < 0, NEGATIVE, 0.0).astype(F32))
+                block = k_all[place_of(jnp.maximum(pick, 0))]
+            else:
+                block = k_all[own_place(k, jb)]
+            nothing = jnp.zeros_like(block)
+            kg[u, j * BLK : j * BLK + half_blk, :] = jnp.where(left_half, block, nothing)
+            kg[u, j * BLK + half_blk : j * BLK + BLK, :] = jnp.where(left_half, nothing, block)
+        return bias
+
+    def score(k, jb, u):
         rows = pl.ds(pl.multiple_of(jb * BLK, BLK), BLK)
         heads = []
         for n in range(2):
@@ -307,55 +348,67 @@
             swapped = pltpu.roll(x, 64, 1)
             heads += [jnp.where(left, x, swapped), jnp.where(left, swapped, x)]
         q2 = jnp.concatenate(heads, axis=0).astype(BF)
-        bias = []
+        scores[u] = lax.dot_general(
+            kg[u], q2, (((1,), (1,)), ((), ())), preferred_element_type=F32
+        )
+
+    def softmax(k, jb, u, bias):
+        def rows_of(j):
+            return scores[u, j * BLK : j * BLK + BLK, :]
+
+        def eight(x, op):
+            return op(x.reshape(BLK // 8, 8, 4 * BLK), axis=0)
+
+        tail = jnp.where(causal, rows_of(PICK), NEGATIVE)
+        top = eight(tail, jnp.max)
+        for j in range(PICK):
+            top = jnp.maximum(top, eight(rows_of(j), jnp.max) + bias[j])
+        top = jnp.max(top, axis=0, keepdims=True)
+        total = jnp.zeros((8, 4 * BLK), F32)
         for j in range(PICK + 1):
-            if j < PICK:
-                pick = ch_smem[k, t * 4 + jb, j]
-                bias.append(jnp.where(pick < 0, NEGATIVE, 0.0).astype(F32))
-                block = k_all[jnp.maximum(pick, 0)]
-            else:
-                block = k_all[own_block(k, jb)]
-            nothing = jnp.zeros_like(block)
-            kg[j * BLK : j * BLK + half_blk, :] = jnp.where(left_half, block, nothing)
-            kg[j * BLK + half_blk : j * BLK + BLK, :] = jnp.where(left_half, nothing, block)
-        scores[...] = lax.dot_general(
-            kg[...], q2, (((1,), (1,)), ((), ())), preferred_element_type=F32
-        )
-        tail = jnp.where(causal, scores[PICK * BLK :, :], NEGATIVE)
-        top = jnp.max(tail, axis=0, keepdims=True)
-        for j in range(PICK):
-            here = jnp.max(scores[j * BLK : j * BLK + BLK, :], axis=0, keepdims=True)
-            top = jnp.maximum(top, here + bias[j])
-        total = jnp.zeros((1, 4 * BLK), F32)
-        for j in range(PICK + 1):
-            s = tail if j == PICK else scores[j * BLK : j * BLK + BLK, :]
+            s = tail if j == PICK else rows_of(j)
             shift = top if j == PICK else top - bias[j]
             p = jnp.exp2((s - shift) * EXPONENT)
-            total = total + jnp.sum(p, axis=0, keepdims=True)
+            total = total + eight(p, jnp.sum)
             probs[k * 4 + jb, j * BLK : j * BLK + BLK, :] = p.astype(BF)
+        total = jnp.sum(total, axis=0, keepdims=True)
         inverse[k, pl.ds(jb, 1), :] = 1.0 / total
         ls_out[k, pl.ds(jb, 1), :] = top * HEAD_DIM**-0.5 + jnp.log(total)
 
-    def combine(k, jb):
-        rows = pl.ds(pl.multiple_of(jb * BLK, BLK), BLK)
+    def weigh(k, pair):
+        blocks = [(k, 2 * pair + u, u) for u in range(2)]
+        bias = [gather_keys(*block) for block in blocks]
+        for block in blocks:
+            score(*block)
+        for block in blocks:
+            softmax(*block, bias[block[2]])
+
+    def gather_values(k, jb):
         previous = None
         for j in range(PICK + 1):
             if j < PICK:
-                block = v_all[jnp.maximum(ch_smem[k, t * 4 + jb, j], 0)]
+                block = v_all[place_of(jnp.maximum(ch_smem[k, t * 4 + jb, j], 0))]
             else:
-                block = v_all[own_block(k, jb)]
+                block = v_all[own_place(k, jb)]
             block = block.astype(F32)
             if j % 2 == 1:
                 low = jnp.where(left_half, previous, pltpu.roll(block, 64, 1))
                 high = jnp.where(left_half, pltpu.roll(previous, 64, 1), block)
                 columns = slice((j // 2) * 128, (j // 2) * 128 + 128)
-                vt[:half_blk, columns] = low.astype(BF)
-                vt[half_blk:, columns] = high.astype(BF)
+                vt[jb, :half_blk, columns] = low.astype(BF)
+                vt[jb, half_blk:, columns] = high.astype(BF)
             previous = block
-        mixed = jnp.dot(vt[...], probs[k * 4 + jb], preferred_element_type=F32)
-        turned_back = (mixed * inverse[k, pl.ds(jb, 1), :]).T
-        parts = [turned_back[h * BLK : h * BLK + BLK] for h in range(4)]
-        att_out[k, rows, :] = jnp.concatenate(parts, axis=1).astype(BF)
+
+    def combine(k):
+        for jb in range(4):
+            gather_values(k, jb)
+        mixed = [
+            jnp.dot(vt[jb], probs[k * 4 + jb], preferred_element_type=F32) for jb in range(4)
+        ]
+        for jb in range(4):
+            turned_back = (mixed[jb] * inverse[k, jb : jb + 1, :]).T
+            parts = [turned_back[h * BLK : h * BLK + BLK] for h in range(4)]
+            att_out[k, jb * BLK : jb * BLK + BLK, :] = jnp.concatenate(parts, axis=1).astype(BF)
 
     to_self = y // 2 == t
     slot = (lax.rem(y, 2), t)
@@ -366,10 +419,10 @@
         )
 
     for s, k in enumerate((2, 1, 3, 0)):
-        @pl.loop(0, 4)
-        def _(jb):
-            weigh(k, jb)
-            step(v_ring, s + 1, jb)
+        @pl.loop(0, 2)
+        def _(pair):
+            weigh(k, pair)
+            step(v_ring, s + 1, pair)
 
         if k > 0:
             log_piece(k).start()
@@ -381,15 +434,12 @@
                 ls_ref[slot] = ls_out[0]
 
     for rel in range(NZ):
-        for k in range(NY):
-            v_ring[2](rel, k).wait_recv()
+        for c in range(2):
+            v_ring[2](rel, c).wait_recv()
 
     back = {}
     for k in (2, 1, 3, 0):
-        @pl.loop(0, 4)
-        def _(jb):
-            combine(k, jb)
-
+        combine(k)
         if k > 0:
             back[NY - k] = remote(
                 att_out.at[k], att_all.at[NY - k], a_send.at[k], a_recv.at[NY - k],
@@ -433,14 +483,17 @@
     for copy in halves + picks:
         copy.wait_send()
     for up, down, partner in (k_ring, v_ring):
-        for k in range(NY):
-            for s in range(NZ // 2):
-                if s < NZ // 2 - 1 or k < 2:
-                    up(s, k).wait_send()
-                if s < NZ // 2 - 1 or k >= 2:
-                    down(s, k).wait_send()
+        for r in range(NY):
+            up(0, r).wait_send()
+            down(0, r).wait_send()
+        for c in range(2):
+            for s in range(1, NZ // 2):
+                if s < NZ // 2 - 1 or c == 0:
+                    up(s, c).wait_send()
+                if s < NZ // 2 - 1 or c == 1:
+                    down(s, c).wait_send()
             for rel in range(NZ):
-                partner(rel, k).wait_send()
+                partner(rel, c).wait_send()
 
 
 def shards(tokens, w_query, w_key, w_value, w_out, chosen):
@@ -477,9 +530,9 @@
             pltpu.VMEM((NY, rows, 256), BF),
             pltpu.VMEM((NY, 8, PICK), jnp.int32),
             pltpu.SMEM((NY, 8, PICK), jnp.int32),
-            pltpu.VMEM(((PICK + 1) * BLK, 128), BF),
-            pltpu.VMEM((BLK, (PICK + 1) * BLK), BF),
-            pltpu.VMEM(((PICK + 1) * BLK, 4 * BLK), F32),
+            pltpu.VMEM((2, (PICK + 1) * BLK, 128), BF),
+            pltpu.VMEM((4, BLK, (PICK + 1) * BLK), BF),
+            pltpu.VMEM((2, (PICK + 1) * BLK, 4 * BLK), F32),
             pltpu.VMEM((NY * 4, (PICK + 1) * BLK, 4 * BLK), BF),
             pltpu.VMEM((NY, 4, 4 * BLK), F32),
             pltpu.VMEM((NY, rows, 256), BF),
@@ -487,8 +540,10 @@
             pltpu.VMEM((NY, 4, 4 * BLK), F32),
             pltpu.VMEM((rows, width), F32),
             dma((14,)), dma((4,)), dma((4,)), dma((4,)), dma((4,)), dma((4,)), dma((4,)),
-            dma((4, 4)), dma((4, 4)), dma((4, 4)), dma((4, 4)), dma((NZ, 4)), dma((NZ, 4)),
-            dma((4, 4)), dma((4, 4)), dma((4, 4)), dma((4, 4)), dma((NZ, 4)), dma((NZ, 4)),
+            dma((2, 4)), dma((2, 4)), dma((4, 2)), dma((4, 2)), dma((4, 2)), dma((4, 2)),
+            dma((NZ, 2)), dma((NZ, 2)),
+            dma((2, 4)), dma((2, 4)), dma((4, 2)), dma((4, 2)), dma((4, 2)), dma((4, 2)),
+            dma((NZ, 2)), dma((NZ, 2)),
             dma((4,)), dma((4,)), dma((4,)), dma((4,)),
             dma((4,)), dma((4,)), dma((4,)), dma((2, 2)),
         ],

time: 63.7 us -> 63.1 us (level)
  no operation moved by 1% of the time
where the time goes in v3:
time: 63.1 us; the launch traced here: 63 us
  Pallas kernels  58.9 us (93%)
  local copies, waits for them, and re-layouts  3.37 us (5%)
  between operations  0.65 us (1%)
    pallas_call x1, Pallas kernels, shards(): pl.pallas_call(kernel, out_shape=(jax.ShapeDtypeStruct((rows, width), BF)...  58.9 us
    unnamed x1, local copies, waits for them, and re-layouts  1.87 us

profile of v3, /device:TPU:1, one launch (start us, length us, event | category | flops | bytes accessed | tf_op | source)
XLA Modules:
  0.0 63.0 jit_solution(4733249054140983328)
XLA Ops:
  0.6 58.9 %shard_map.113 = (bf16[256,1024]{1,0:T(8,128)(2,1)}, f32[2,2,4,256]{3,2,1,0:T(4,128)}) custom-call(f32[256,128]{1,0:T(8,128)} %constant.8.clone.cr_hbm, f32[256,128]{1,0:T(8,128)} %constant.9.clone.sr_hbm, f32[64,128]{1,0:T(8,128)} %constant.10.clone.cb_hbm, f32[64,128]{1,0:T(8,128)} %constant.11.clone.sb_hbm, bf16[256,1024]{1,0:T(8,128)(2,1)} %bitcast.7, ...), custom_call_target="tpu_custom_call" | custom-call | tf_op jit(solution)/shard_map/pallas_call | solution.py:505
  59.6 0.8 %reshape.7 = f32[2,2,4,4,64]{4,3,2,1,0:T(4,128)S(1)} reshape(f32[2,2,4,256]{3,2,1,0:T(4,128)} %get-tuple-element.5) | data formatting | bytes 32768 | tf_op jit(solution)/shard_map/reshape | solution.py:554
  60.4 0.7 %broadcast_in_dim_reshape.3 = f32[1,512,8]{1,2,0:T(8,128)} reshape(f32[2,4,64,2,4]{2,1,0,4,3:T(4,128)S(1)} %copy.12) | data formatting | bytes 32768 | tf_op jit(solution)/shard_map/broadcast_in_dim;reshape | solution.py:555
  61.1 1.9 %copy.14 = bf16[1,256,1024]{2,1,0:T(8,128)(2,1)} copy(bf16[1,256,1024]{2,1,0:T(8,128)(2,1)} %bitcast.6) | data formatting | bytes 1048576
  (1 shorter events, 0.0 us)

commit v4 on v2

--- a/solution.py
+++ b/solution.py
@@ -143,8 +143,8 @@
     pl.semaphore_wait(barrier, len(peers))
 
     halves = [
-        remote(wk_hbm, wk.at[t], w_send.at[0], w_recv.at[0], kv, other),
-        remote(wv_hbm, wv.at[t], w_send.at[1], w_recv.at[1], kv, other),
+        remote(wk.at[t], wk.at[t], w_send.at[0], w_recv.at[0], kv, other),
+        remote(wv.at[t], wv.at[t], w_send.at[1], w_recv.at[1], kv, other),
         remote(wq_hbm, wq.at[t], w_send.at[2], w_recv.at[2], kv, other),
         remote(wo_hbm, wo.at[t], w_send.at[3], w_recv.at[3], kv, other),
     ]
@@ -263,26 +263,28 @@
             row_peer(k), t,
         ).wait_recv()
 
-    for k in (1, 3, 2):
-        from_row(k_all, k_own, ky_send, ky_recv, k)
-        begin(k_ring, k)
-    for s in range(1, NZ // 2):
-        for k in range(NY):
-            step(k_ring, s, k)
-    for copy in mine:
-        copy.wait()
-    begin(v_ring, 0)
-    for k in (1, 2, 3):
-        from_row(v_all, v_own, vy_send, vy_recv, k)
-        begin(v_ring, k)
-    for k in range(NY):
-        step(k_ring, NZ // 2, k)
-
     for copy in picks:
         copy.wait_recv()
     own_picks.wait()
     to_smem = pltpu.make_async_copy(ch_all, ch_smem, load_sem.at[13])
     to_smem.start()
+    for k in (1, 3, 2):
+        from_row(k_all, k_own, ky_send, ky_recv, k)
+        begin(k_ring, k)
+    for copy in mine:
+        copy.wait()
+    begin(v_ring, 0)
+    for k in (1, 3, 2):
+        from_row(v_all, v_own, vy_send, vy_recv, k)
+        begin(v_ring, k)
+    order = (0, 1, 3, 2)
+    for s in range(1, NZ // 2 + 1):
+        for k in order:
+            step(k_ring, s, k)
+        if s > 1 and s <= NZ // 2 - 1:
+            for k in order:
+                step(v_ring, s - 1, k)
+
     to_smem.wait()
     own_q.wait()
     for k in range(1, NY):
@@ -299,14 +301,7 @@
     def own_block(k, jb):
         return (z * NY + row_chip(k)) * 8 + t * 4 + jb
 
-    def weigh(k, jb):
-        rows = pl.ds(pl.multiple_of(jb * BLK, BLK), BLK)
-        heads = []
-        for n in range(2):
-            x = q_all[k, rows, n * 128 : n * 128 + 128].astype(F32)
-            swapped = pltpu.roll(x, 64, 1)
-            heads += [jnp.where(left, x, swapped), jnp.where(left, swapped, x)]
-        q2 = jnp.concatenate(heads, axis=0).astype(BF)
+    def gather_keys(k, jb):
         bias = []
         for j in range(PICK + 1):
             if j < PICK:
@@ -316,28 +311,70 @@
             else:
                 block = k_all[own_block(k, jb)]
             nothing = jnp.zeros_like(block)
-            kg[j * BLK : j * BLK + half_blk, :] = jnp.where(left_half, block, nothing)
-            kg[j * BLK + half_blk : j * BLK + BLK, :] = jnp.where(left_half, nothing, block)
-        scores[...] = lax.dot_general(
-            kg[...], q2, (((1,), (1,)), ((), ())), preferred_element_type=F32
-        )
-        tail = jnp.where(causal, scores[PICK * BLK :, :], NEGATIVE)
-        top = jnp.max(tail, axis=0, keepdims=True)
-        for j in range(PICK):
-            here = jnp.max(scores[j * BLK : j * BLK + BLK, :], axis=0, keepdims=True)
-            top = jnp.maximum(top, here + bias[j])
-        total = jnp.zeros((1, 4 * BLK), F32)
-        for j in range(PICK + 1):
-            s = tail if j == PICK else scores[j * BLK : j * BLK + BLK, :]
+            u, row = jb % 2, j * BLK
+            kg[u, row : row + half_blk, :] = jnp.where(left_half, block, nothing)
+            kg[u, row + half_blk : row + BLK, :] = jnp.where(left_half, nothing, block)
+        return bias
+
+    def load_queries(k, jb):
+        heads = []
+        for n in range(2):
+            x = q_all[k, jb * BLK : jb * BLK + BLK, n * 128 : n * 128 + 128].astype(F32)
+            swapped = pltpu.roll(x, 64, 1)
+            heads += [jnp.where(left, x, swapped), jnp.where(left, swapped, x)]
+        return jnp.concatenate(heads, axis=0).astype(BF)
+
+    def eight(x, op):
+        return op(x.reshape(BLK // 8, 8, 4 * BLK), axis=0)
+
+    def score(u, half, q2, bias):
+        span = 8 * BLK
+        part = lax.dot_general(
+            kg[u, half * span : half * span + span, :], q2, (((1,), (1,)), ((), ())),
+            preferred_element_type=F32,
+        )
+        top = None
+        for i in range(8):
+            j = half * 8 + i
+            block = part[i * BLK : i * BLK + BLK, :]
+            if j == PICK:
+                block = jnp.where(causal, block, NEGATIVE)
+            scores[u, j * BLK : j * BLK + BLK, :] = block
+            here = eight(block, jnp.max)
+            here = here if j == PICK else here + bias[j]
+            top = here if top is None else jnp.maximum(top, here)
+        return top
+
+    def softmax(state, half):
+        k, jb, top, bias, total = state
+        for j in range(half * 8, half * 8 + 8):
             shift = top if j == PICK else top - bias[j]
-            p = jnp.exp2((s - shift) * EXPONENT)
-            total = total + jnp.sum(p, axis=0, keepdims=True)
-            probs[k * 4 + jb, j * BLK : j * BLK + BLK, :] = p.astype(BF)
-        inverse[k, pl.ds(jb, 1), :] = 1.0 / total
-        ls_out[k, pl.ds(jb, 1), :] = top * HEAD_DIM**-0.5 + jnp.log(total)
-
-    def combine(k, jb):
-        rows = pl.ds(pl.multiple_of(jb * BLK, BLK), BLK)
+            p = jnp.exp2((scores[jb % 2, j * BLK : j * BLK + BLK, :] - shift) * EXPONENT)
+            part = eight(p, jnp.sum)
+            total = part if total is None else total + part
+            probs[jb, j * BLK : j * BLK + BLK, :] = p.astype(BF)
+        if half == 1:
+            total = jnp.sum(total, axis=0, keepdims=True)
+            inverse[k, pl.ds(jb, 1), :] = 1.0 / total
+            ls_out[k, pl.ds(jb, 1), :] = top * HEAD_DIM**-0.5 + jnp.log(total)
+        return k, jb, top, bias, total
+
+    def weigh(k):
+        state = None
+        for jb in range(4):
+            bias = gather_keys(k, jb)
+            q2 = load_queries(k, jb)
+            tops = []
+            for half in range(2):
+                tops.append(score(jb % 2, half, q2, bias))
+                if state is not None:
+                    state = softmax(state, half)
+            top = jnp.max(jnp.maximum(*tops), axis=0, keepdims=True)
+            state = (k, jb, top, bias, None)
+        for half in range(2):
+            state = softmax(state, half)
+
+    def gather_values(k, jb):
         previous = None
         for j in range(PICK + 1):
             if j < PICK:
@@ -349,13 +386,20 @@
                 low = jnp.where(left_half, previous, pltpu.roll(block, 64, 1))
                 high = jnp.where(left_half, pltpu.roll(previous, 64, 1), block)
                 columns = slice((j // 2) * 128, (j // 2) * 128 + 128)
-                vt[:half_blk, columns] = low.astype(BF)
-                vt[half_blk:, columns] = high.astype(BF)
+                vt[jb, :half_blk, columns] = low.astype(BF)
+                vt[jb, half_blk:, columns] = high.astype(BF)
             previous = block
-        mixed = jnp.dot(vt[...], probs[k * 4 + jb], preferred_element_type=F32)
-        turned_back = (mixed * inverse[k, pl.ds(jb, 1), :]).T
-        parts = [turned_back[h * BLK : h * BLK + BLK] for h in range(4)]
-        att_out[k, rows, :] = jnp.concatenate(parts, axis=1).astype(BF)
+
+    def combine(k):
+        for jb in range(4):
+            gather_values(k, jb)
+        mixed = [
+            jnp.dot(vt[jb], probs[jb], preferred_element_type=F32) for jb in range(4)
+        ]
+        for jb in range(4):
+            turned_back = (mixed[jb] * inverse[k, pl.ds(jb, 1), :]).T
+            parts = [turned_back[h * BLK : h * BLK + BLK] for h in range(4)]
+            att_out[k, jb * BLK : jb * BLK + BLK, :] = jnp.concatenate(parts, axis=1).astype(BF)
 
     to_self = y // 2 == t
     slot = (lax.rem(y, 2), t)
@@ -365,43 +409,43 @@
             ls_out.at[k], ls_ref.at[slot], l_send.at[k], l_recv.at[slot], row_peer(k), y // 2
         )
 
-    for s, k in enumerate((2, 1, 3, 0)):
-        @pl.loop(0, 4)
-        def _(jb):
-            weigh(k, jb)
-            step(v_ring, s + 1, jb)
-
-        if k > 0:
+    def give_back(k):
+        return remote(
+            att_out.at[k], att_all.at[NY - k], a_send.at[k], a_recv.at[NY - k], row_peer(k), t
+        )
+
+    @pl.loop(0, NY)
+    def _(i):
+        k = lax.rem(i + 1, NY)
+        weigh(k)
+
+        @pl.when(i == 0)
+        def _():
+            for s in (NZ // 2 - 1, NZ // 2):
+                for r in order:
+                    step(v_ring, s, r)
+            for rel in range(NZ):
+                for r in range(NY):
+                    v_ring[2](rel, r).wait_recv()
+
+        combine(k)
+
+        @pl.when(k > 0)
+        def _():
+            give_back(k).start()
             log_piece(k).start()
-        else:
-            pl.when(jnp.logical_not(to_self))(lambda: log_piece(0).start())
-
-            @pl.when(to_self)
-            def _():
-                ls_ref[slot] = ls_out[0]
-
-    for rel in range(NZ):
-        for k in range(NY):
-            v_ring[2](rel, k).wait_recv()
-
-    back = {}
-    for k in (2, 1, 3, 0):
-        @pl.loop(0, 4)
-        def _(jb):
-            combine(k, jb)
-
-        if k > 0:
-            back[NY - k] = remote(
-                att_out.at[k], att_all.at[NY - k], a_send.at[k], a_recv.at[NY - k],
-                row_peer(k), t,
-            )
-            back[NY - k].start()
+
+    pl.when(jnp.logical_not(to_self))(lambda: log_piece(0).start())
+
+    @pl.when(to_self)
+    def _():
+        ls_ref[slot] = ls_out[0]
 
     loads[4].wait()
     halves[3].wait_recv()
     for k in (0, 1, 3, 2):
         if k > 0:
-            back[k].wait_recv()
+            give_back(NY - k).wait_recv()
         ys = row_chip(k)
         weights = wo[ys // 2, pl.ds(pl.multiple_of(lax.rem(ys, 2) * 256, 256), 256), :]
         piece = att_out[0] if k == 0 else att_all[k]
@@ -429,7 +473,7 @@
         key_to_owner(row_chip(k)).wait_send()
         value_to_owner(row_chip(k)).wait_send()
         queries[k].wait_send()
-        back[k].wait_send()
+        give_back(k).wait_send()
     for copy in halves + picks:
         copy.wait_send()
     for up, down, partner in (k_ring, v_ring):
@@ -477,10 +521,10 @@
             pltpu.VMEM((NY, rows, 256), BF),
             pltpu.VMEM((NY, 8, PICK), jnp.int32),
             pltpu.SMEM((NY, 8, PICK), jnp.int32),
-            pltpu.VMEM(((PICK + 1) * BLK, 128), BF),
-            pltpu.VMEM((BLK, (PICK + 1) * BLK), BF),
-            pltpu.VMEM(((PICK + 1) * BLK, 4 * BLK), F32),
-            pltpu.VMEM((NY * 4, (PICK + 1) * BLK, 4 * BLK), BF),
+            pltpu.VMEM((2, (PICK + 1) * BLK, 128), BF),
+            pltpu.VMEM((4, BLK, (PICK + 1) * BLK), BF),
+            pltpu.VMEM((2, (PICK + 1) * BLK, 4 * BLK), F32),
+            pltpu.VMEM((4, (PICK + 1) * BLK, 4 * BLK), BF),
             pltpu.VMEM((NY, 4, 4 * BLK), F32),
             pltpu.VMEM((NY, rows, 256), BF),
             pltpu.VMEM((NY, rows, 256), BF),

time: 63.7 us -> 58.3 us (0.915)
  Pallas kernels: 59.5 us -> 53.5 us
    pallas_call x1, Pallas kernels: 59.5 us -> 53.5 us  [shards(): pl.pallas_call(kernel, out_shape=(jax.ShapeDtypeStruct((rows, width), BF)...]
where the time goes in v4:
time: 58.3 us; the launch traced here: 57.5 us
  Pallas kernels  53.5 us (92%)
  local copies, waits for them, and re-layouts  3.37 us (6%)
  between operations  0.65 us (1%)
    pallas_call x1, Pallas kernels, shards(): pl.pallas_call(kernel, out_shape=(jax.ShapeDtypeStruct((rows, width), BF)...  53.5 us
    unnamed x1, local copies, waits for them, and re-layouts  1.87 us

profile of v4, /device:TPU:1, one launch (start us, length us, event | category | flops | bytes accessed | tf_op | source)
XLA Modules:
  0.0 57.5 jit_solution(6924460788857789974)
XLA Ops:
  0.6 53.5 %shard_map.113 = (bf16[256,1024]{1,0:T(8,128)(2,1)}, f32[2,2,4,256]{3,2,1,0:T(4,128)}) custom-call(f32[256,128]{1,0:T(8,128)} %constant.8.clone.cr_hbm, f32[256,128]{1,0:T(8,128)} %constant.9.clone.sr_hbm, f32[64,128]{1,0:T(8,128)} %constant.10.clone.cb_hbm, f32[64,128]{1,0:T(8,128)} %constant.11.clone.sb_hbm, bf16[256,1024]{1,0:T(8,128)(2,1)} %bitcast.7, ...), custom_call_target="tpu_custom_call" | custom-call | tf_op jit(solution)/shard_map/pallas_call | solution.py:496
  54.2 0.8 %reshape.7 = f32[2,2,4,4,64]{4,3,2,1,0:T(4,128)S(1)} reshape(f32[2,2,4,256]{3,2,1,0:T(4,128)} %get-tuple-element.5) | data formatting | bytes 32768 | tf_op jit(solution)/shard_map/reshape | solution.py:543
  55.0 0.7 %broadcast_in_dim_reshape.3 = f32[1,512,8]{1,2,0:T(8,128)} reshape(f32[2,4,64,2,4]{2,1,0,4,3:T(4,128)S(1)} %copy.12) | data formatting | bytes 32768 | tf_op jit(solution)/shard_map/broadcast_in_dim;reshape | solution.py:544
  55.7 1.9 %copy.14 = bf16[1,256,1024]{2,1,0:T(8,128)(2,1)} copy(bf16[1,256,1024]{2,1,0:T(8,128)(2,1)} %bitcast.6) | data formatting | bytes 1048576
  (1 shorter events, 0.0 us)

commit v5 on v4

--- a/solution.py
+++ b/solution.py
@@ -39,7 +39,7 @@
     out_ref, ls_ref,
     cr_ref, sr_ref, cb_ref, sb_ref, tok, wq, wk, wv, wo, cosine, sine, k_own, v_own,
     k_all, v_all, qs, q_all, ch_all, ch_smem, kg, vt, scores, probs, inverse,
-    att_out, att_all, ls_out, acc,
+    att_out, att_all, ls_out, ls_all, acc,
     load_sem, w_send, w_recv, ky_send, ky_recv, vy_send, vy_recv,
     k_up_send, k_up_recv, k_dn_send, k_dn_recv, k_pt_send, k_pt_recv,
     v_up_send, v_up_recv, v_dn_send, v_dn_recv, v_pt_send, v_pt_recv,
@@ -111,19 +111,22 @@
         swapped = jnp.where(first, pltpu.roll(x, 96, 1), pltpu.roll(x, 32, 1))
         return x * cosine[...] + swapped * sine[...]
 
-    def project_kv(half):
-        tokens = tok[...]
-        keys = jnp.dot(tokens, wk[half], preferred_element_type=F32).astype(BF).astype(F32)
+    def project_k(half):
+        keys = jnp.dot(tok[...], wk[half], preferred_element_type=F32).astype(BF).astype(F32)
         keys = rotate(keys)
         keys = (keys, pltpu.roll(keys, 64, 1))
-        values = jnp.dot(tokens, wv[half], preferred_element_type=F32).T
-        values = [values[:, i * 128 : i * 128 + 128] for i in range(2)]
-        values = [(x, pltpu.roll(x, 64, 1)) for x in values]
         for e in range(2):
             for j in range(4):
                 low = keys[e][j * 64 : j * 64 + 32]
                 high = keys[1 - e][j * 64 + 32 : j * 64 + 64]
                 k_own[2 * half + e, j] = jnp.where(left_half, low, high).astype(BF)
+
+    def project_v(half):
+        values = jnp.dot(tok[...], wv[half], preferred_element_type=F32).T
+        values = [values[:, i * 128 : i * 128 + 128] for i in range(2)]
+        values = [(x, pltpu.roll(x, 64, 1)) for x in values]
+        for e in range(2):
+            for j in range(4):
                 pair = values[j // 2]
                 low = pair[j % 2][e * 64 : e * 64 + 32]
                 high = pair[1 - j % 2][e * 64 + 32 : e * 64 + 64]
@@ -138,14 +141,15 @@
 
     for load in loads[:3]:
         load.wait()
-    project_kv(t)
+    project_k(t)
+    project_v(t)
 
     pl.semaphore_wait(barrier, len(peers))
 
     halves = [
         remote(wk.at[t], wk.at[t], w_send.at[0], w_recv.at[0], kv, other),
         remote(wv.at[t], wv.at[t], w_send.at[1], w_recv.at[1], kv, other),
-        remote(wq_hbm, wq.at[t], w_send.at[2], w_recv.at[2], kv, other),
+        remote(wq.at[t], wq.at[t], w_send.at[2], w_recv.at[2], kv, other),
         remote(wo_hbm, wo.at[t], w_send.at[3], w_recv.at[3], kv, other),
     ]
 
@@ -160,31 +164,27 @@
     def value_to_owner(head):
         return to_owner(v_own, v_all, vy_send, vy_recv, head)
 
-    def send_heads(half):
-        for make in (key_to_owner, value_to_owner):
-            for e in range(2):
-                head = 2 * half + e
-
-                @pl.when(head != y)
-                def _():
-                    make(head).start()
+    def send_heads(make, half):
+        for e in range(2):
+            head = 2 * half + e
+
+            @pl.when(head != y)
+            def _():
+                make(head).start()
 
     for copy in halves[:2]:
         copy.start()
-    send_heads(t)
+    send_heads(key_to_owner, t)
     picks = [
         remote(ch_hbm, ch_all.at[NY - k], c_send.at[k], c_recv.at[NY - k], row_peer(k), t)
         for k in range(1, NY)
     ]
+    loads[3].wait()
     for copy in halves[2:] + picks:
         copy.start()
-
-    loads[3].wait()
-    project_q(t)
-    for copy in halves[:2]:
-        copy.wait_recv()
-    project_kv(other)
-    send_heads(other)
+    halves[0].wait_recv()
+    project_k(other)
+    send_heads(key_to_owner, other)
 
     def ring(every, up_send, up_recv, dn_send, dn_recv, pt_send, pt_recv):
         def place(zz, k):
@@ -242,9 +242,29 @@
         pltpu.make_async_copy(v_own.at[y], v_all.at[chunk(z, y)], load_sem.at[7]),
     ]
     begin(k_ring, 0, k_own.at[y])
+    send_heads(value_to_owner, t)
+    halves[1].wait_recv()
+    project_v(other)
+    send_heads(value_to_owner, other)
     for copy in mine:
         copy.start()
 
+    def from_row(every, own, send, recv, k):
+        remote(
+            own.at[0], every.at[chunk(z, row_chip(k))], send.at[0], recv.at[row_chip(k)],
+            row_peer(k), t,
+        ).wait_recv()
+
+    for k in (1, 3, 2):
+        from_row(k_all, k_own, ky_send, ky_recv, k)
+        begin(k_ring, k)
+    for copy in mine:
+        copy.wait()
+    begin(v_ring, 0)
+    for k in (1, 3, 2):
+        from_row(v_all, v_own, vy_send, vy_recv, k)
+        begin(v_ring, k)
+    project_q(t)
     halves[2].wait_recv()
     project_q(other)
     own_q = pltpu.make_async_copy(qs.at[y], q_all.at[0], load_sem.at[6])
@@ -257,33 +277,19 @@
         )
         queries[NY - k].start()
 
-    def from_row(every, own, send, recv, k):
-        remote(
-            own.at[0], every.at[chunk(z, row_chip(k))], send.at[0], recv.at[row_chip(k)],
-            row_peer(k), t,
-        ).wait_recv()
-
     for copy in picks:
         copy.wait_recv()
     own_picks.wait()
     to_smem = pltpu.make_async_copy(ch_all, ch_smem, load_sem.at[13])
     to_smem.start()
-    for k in (1, 3, 2):
-        from_row(k_all, k_own, ky_send, ky_recv, k)
-        begin(k_ring, k)
-    for copy in mine:
-        copy.wait()
-    begin(v_ring, 0)
-    for k in (1, 3, 2):
-        from_row(v_all, v_own, vy_send, vy_recv, k)
-        begin(v_ring, k)
+
     order = (0, 1, 3, 2)
     for s in range(1, NZ // 2 + 1):
         for k in order:
             step(k_ring, s, k)
-        if s > 1 and s <= NZ // 2 - 1:
+        if s < NZ // 2:
             for k in order:
-                step(v_ring, s - 1, k)
+                step(v_ring, s, k)
 
     to_smem.wait()
     own_q.wait()
@@ -356,7 +362,9 @@
         if half == 1:
             total = jnp.sum(total, axis=0, keepdims=True)
             inverse[k, pl.ds(jb, 1), :] = 1.0 / total
-            ls_out[k, pl.ds(jb, 1), :] = top * HEAD_DIM**-0.5 + jnp.log(total)
+            logsum = top * HEAD_DIM**-0.5 + jnp.log(total)
+            for h in range(4):
+                ls_out[k, pl.ds(h, 1), jb * BLK : jb * BLK + BLK] = logsum[:, h * BLK : h * BLK + BLK]
         return k, jb, top, bias, total
 
     def weigh(k):
@@ -406,7 +414,7 @@
 
     def log_piece(k):
         return remote(
-            ls_out.at[k], ls_ref.at[slot], l_send.at[k], l_recv.at[slot], row_peer(k), y // 2
+            ls_out.at[k], ls_all.at[slot], l_send.at[k], l_recv.at[slot], row_peer(k), y // 2
         )
 
     def give_back(k):
@@ -421,9 +429,8 @@
 
         @pl.when(i == 0)
         def _():
-            for s in (NZ // 2 - 1, NZ // 2):
-                for r in order:
-                    step(v_ring, s, r)
+            for r in order:
+                step(v_ring, NZ // 2, r)
             for rel in range(NZ):
                 for r in range(NY):
                     v_ring[2](rel, r).wait_recv()
@@ -439,11 +446,11 @@
 
     @pl.when(to_self)
     def _():
-        ls_ref[slot] = ls_out[0]
+        ls_all[slot] = ls_out[0]
 
     loads[4].wait()
     halves[3].wait_recv()
-    for k in (0, 1, 3, 2):
+    for k in (0, 3, 2, 1):
         if k > 0:
             give_back(NY - k).wait_recv()
         ys = row_chip(k)
@@ -452,7 +459,7 @@
         part = jnp.dot(piece, weights, preferred_element_type=F32)
         if k == 0:
             acc[...] = part
-        elif k != 2:
+        elif k != 1:
             acc[...] += part
         else:
             projected = acc[...] + part
@@ -464,8 +471,10 @@
             @pl.when(jnp.logical_not((t * 2 + ys == y) & (t == tt)))
             def _():
                 remote(
-                    ls_out.at[0], ls_ref.at[ys, tt], l_send.at[0], l_recv.at[ys, tt], kv, other
+                    ls_out.at[0], ls_all.at[ys, tt], l_send.at[0], l_recv.at[ys, tt], kv, other
                 ).wait_recv()
+
+            ls_ref[ys * 4 : ys * 4 + 4, tt * 4 * BLK : tt * 4 * BLK + 4 * BLK] = ls_all[ys, tt]
     for k in range(1, NY):
         log_piece(k).wait_send()
     pl.when(jnp.logical_not(to_self))(lambda: log_piece(0).wait_send())
@@ -497,7 +506,7 @@
         kernel,
         out_shape=(
             jax.ShapeDtypeStruct((rows, width), BF),
-            jax.ShapeDtypeStruct((2, 2, 4, 4 * BLK), F32),
+            jax.ShapeDtypeStruct((8, 2 * rows), F32),
         ),
         in_specs=[any_space] * 10,
         out_specs=(vmem, vmem),
@@ -529,6 +538,7 @@
             pltpu.VMEM((NY, rows, 256), BF),
             pltpu.VMEM((NY, rows, 256), BF),
             pltpu.VMEM((NY, 4, 4 * BLK), F32),
+            pltpu.VMEM((2, 2, 4, 4 * BLK), F32),
             pltpu.VMEM((rows, width), F32),
             dma((14,)), dma((4,)), dma((4,)), dma((4,)), dma((4,)), dma((4,)), dma((4,)),
             dma((4, 4)), dma((4, 4)), dma((4, 4)), dma((4, 4)), dma((NZ, 4)), dma((NZ, 4)),
@@ -540,8 +550,7 @@
             collective_id=0, has_side_effects=True, vmem_limit_bytes=67_000_000
         ),
     )(*tables, tokens[0], w_query, w_key, w_value, w_out, chosen[0])
-    logs = logs.reshape(2, 2, 4, 4, BLK).transpose(1, 2, 4, 0, 3).reshape(2 * rows, 8)
-    return out[None], logs[None]
+    return out[None], logs.T[None]
 
 
 def solution(mesh):

time: 58.3 us -> 53.9 us (0.925); the launches traced: 57.5 us -> 53.8 us
  Pallas kernels: 53.5 us -> 50.7 us
  local copies, waits for them, and re-layouts: 3.37 us -> 2.48 us
    pallas_call x1, Pallas kernels: 53.5 us -> 50.7 us  [shards(): pl.pallas_call(kernel, out_shape=(jax.ShapeDtypeStruct((rows, width), BF)...]
    reshape x1 -> x0, local copies, waits for them, and re-layouts: 0.8 us -> none  [shards(): logs.reshape(2, 2, 4, 4, BLK).transpose(1, 2, 4, 0, 3).reshape(2 * rows, 8)]
    another operation x1 -> x0, local copies, waits for them, and re-layouts: 0.69 us -> none  [shards(): return (out[None], logs[None])]
    unnamed x1 -> x4, local copies, waits for them, and re-layouts: 1.87 us -> 2.48 us
where the time goes in v5:
time: 53.9 us; the launch traced here: 53.8 us
  Pallas kernels  50.7 us (94%)
  local copies, waits for them, and re-layouts  2.48 us (5%)
  between operations  0.65 us (1%)
    pallas_call x1, Pallas kernels, shards(): pl.pallas_call(kernel, out_shape=(jax.ShapeDtypeStruct((rows, width), BF)...  50.7 us
    unnamed x4, local copies, waits for them, and re-layouts  2.48 us

profile of v5, /device:TPU:1, one launch (start us, length us, event | category | flops | bytes accessed | tf_op | source)
XLA Modules:
  0.0 53.8 jit_solution(2104312248133080227)
XLA Ops:
  0.6 50.7 %shard_map.113 = (bf16[256,1024]{1,0:T(8,128)(2,1)}, f32[8,512]{1,0:T(8,128)}) custom-call(f32[256,128]{1,0:T(8,128)} %constant.8.clone.cr_hbm, f32[256,128]{1,0:T(8,128)} %constant.9.clone.sr_hbm, f32[64,128]{1,0:T(8,128)} %constant.10.clone.cb_hbm, f32[64,128]{1,0:T(8,128)} %constant.11.clone.sb_hbm, bf16[256,1024]{1,0:T(8,128)(2,1)} %bitcast.7, ...), custom_call_target="tpu_custom_call" | custom-call | tf_op jit(solution)/shard_map/pallas_call | solution.py:505
  51.3 0.0 copy-start
  51.4 1.9 %copy.14 = bf16[1,256,1024]{2,1,0:T(8,128)(2,1)} copy(bf16[1,256,1024]{2,1,0:T(8,128)(2,1)} %bitcast.6) | data formatting | bytes 1048576
  53.2 0.0 copy-done
  53.2 0.6 %copy.15 = f32[1,512,8]{1,2,0:T(8,128)} copy(f32[1,512,8]{1,2,0:T(8,128)S(1)} %bitcast.8) | data formatting | bytes 32768
Async XLA Ops:
  51.3 1.9 %copy-start = (f32[8,512]{1,0:T(8,128)S(1)}, f32[8,512]{1,0:T(8,128)}, u32[]{:S(2)}) copy-start(f32[8,512]{1,0:T(8,128)} %get-tuple-element.5) | copy-start | bytes 49156

commit v6 on v5

--- a/solution.py
+++ b/solution.py
@@ -171,20 +171,6 @@
             @pl.when(head != y)
             def _():
                 make(head).start()
-
-    for copy in halves[:2]:
-        copy.start()
-    send_heads(key_to_owner, t)
-    picks = [
-        remote(ch_hbm, ch_all.at[NY - k], c_send.at[k], c_recv.at[NY - k], row_peer(k), t)
-        for k in range(1, NY)
-    ]
-    loads[3].wait()
-    for copy in halves[2:] + picks:
-        copy.start()
-    halves[0].wait_recv()
-    project_k(other)
-    send_heads(key_to_owner, other)
 
     def ring(every, up_send, up_recv, dn_send, dn_recv, pt_send, pt_recv):
         def place(zz, k):
@@ -237,15 +223,32 @@
             pl.when(k >= 2)(lambda: down(s - 1, k).wait_recv())
             partner(s, k).start()
 
+    for copy in halves[:2]:
+        copy.start()
+    ready = y // 2 == t
+    pl.when(ready)(lambda: begin(k_ring, 0, k_own.at[y]))
+    send_heads(key_to_owner, t)
+    picks = [
+        remote(ch_hbm, ch_all.at[NY - k], c_send.at[k], c_recv.at[NY - k], row_peer(k), t)
+        for k in range(1, NY)
+    ]
+    loads[3].wait()
+    for copy in halves[2:] + picks:
+        copy.start()
+    halves[0].wait_recv()
+    project_k(other)
+    send_heads(key_to_owner, other)
+
     mine = [
         pltpu.make_async_copy(k_own.at[y], k_all.at[chunk(z, y)], load_sem.at[5]),
         pltpu.make_async_copy(v_own.at[y], v_all.at[chunk(z, y)], load_sem.at[7]),
     ]
-    begin(k_ring, 0, k_own.at[y])
+    pl.when(jnp.logical_not(ready))(lambda: begin(k_ring, 0, k_own.at[y]))
     send_heads(value_to_owner, t)
     halves[1].wait_recv()
     project_v(other)
     send_heads(value_to_owner, other)
+    begin(v_ring, 0, v_own.at[y])
     for copy in mine:
         copy.start()
 
@@ -260,7 +263,6 @@
         begin(k_ring, k)
     for copy in mine:
         copy.wait()
-    begin(v_ring, 0)
     for k in (1, 3, 2):
         from_row(v_all, v_own, vy_send, vy_recv, k)
         begin(v_ring, k)
@@ -450,21 +452,19 @@
 
     loads[4].wait()
     halves[3].wait_recv()
-    for k in (0, 3, 2, 1):
-        if k > 0:
-            give_back(NY - k).wait_recv()
+    def part(k):
         ys = row_chip(k)
         weights = wo[ys // 2, pl.ds(pl.multiple_of(lax.rem(ys, 2) * 256, 256), 256), :]
         piece = att_out[0] if k == 0 else att_all[k]
-        part = jnp.dot(piece, weights, preferred_element_type=F32)
-        if k == 0:
-            acc[...] = part
-        elif k != 1:
-            acc[...] += part
-        else:
-            projected = acc[...] + part
-            square = jnp.mean(projected * projected, axis=-1, keepdims=True)
-            out_ref[...] = (projected * lax.rsqrt(square + EPSILON)).astype(BF)
+        return jnp.dot(piece, weights, preferred_element_type=F32)
+
+    for k in (1, 2):
+        give_back(k).wait_recv()
+    acc[...] = part(0) + part(3) + part(2)
+    give_back(3).wait_recv()
+    projected = acc[...] + part(1)
+    square = jnp.mean(projected * projected, axis=-1, keepdims=True)
+    out_ref[...] = (projected * lax.rsqrt(square + EPSILON)).astype(BF)
 
     for ys in range(2):
         for tt in range(2):

time: 53.9 us -> 53.4 us (level)
  Pallas kernels: 50.7 us -> 50.1 us
    pallas_call x1, Pallas kernels: 50.7 us -> 50.1 us  [shards(): pl.pallas_call(kernel, out_shape=(jax.ShapeDtypeStruct((rows, width), BF)...]
where the time goes in v6:
time: 53.4 us; the launch traced here: 53.3 us
  Pallas kernels  50.1 us (94%)
  local copies, waits for them, and re-layouts  2.48 us (5%)
  between operations  0.65 us (1%)
    pallas_call x1, Pallas kernels, shards(): pl.pallas_call(kernel, out_shape=(jax.ShapeDtypeStruct((rows, width), BF)...  50.1 us
    unnamed x4, local copies, waits for them, and re-layouts  2.48 us

profile of v6, /device:TPU:1, one launch (start us, length us, event | category | flops | bytes accessed | tf_op | source)
XLA Modules:
  0.0 53.3 jit_solution(16044872637946522301)
XLA Ops:
  0.6 50.1 %shard_map.113 = (bf16[256,1024]{1,0:T(8,128)(2,1)}, f32[8,512]{1,0:T(8,128)}) custom-call(f32[256,128]{1,0:T(8,128)} %constant.8.clone.cr_hbm, f32[256,128]{1,0:T(8,128)} %constant.9.clone.sr_hbm, f32[64,128]{1,0:T(8,128)} %constant.10.clone.cb_hbm, f32[64,128]{1,0:T(8,128)} %constant.11.clone.sb_hbm, bf16[256,1024]{1,0:T(8,128)(2,1)} %bitcast.7, ...), custom_call_target="tpu_custom_call" | custom-call | tf_op jit(solution)/shard_map/pallas_call | solution.py:505
  50.8 0.0 copy-start
  50.8 1.9 %copy.14 = bf16[1,256,1024]{2,1,0:T(8,128)(2,1)} copy(bf16[1,256,1024]{2,1,0:T(8,128)(2,1)} %bitcast.6) | data formatting | bytes 1048576
  52.6 0.0 copy-done
  52.6 0.6 %copy.15 = f32[1,512,8]{1,2,0:T(8,128)} copy(f32[1,512,8]{1,2,0:T(8,128)S(1)} %bitcast.8) | data formatting | bytes 32768
Async XLA Ops:
  50.8 1.9 %copy-start = (f32[8,512]{1,0:T(8,128)S(1)}, f32[8,512]{1,0:T(8,128)}, u32[]{:S(2)}) copy-start(f32[8,512]{1,0:T(8,128)} %get-tuple-element.5) | copy-start | bytes 49156

commit v7 on v6

--- a/solution.py
+++ b/solution.py
@@ -426,7 +426,7 @@
 
     @pl.loop(0, NY)
     def _(i):
-        k = lax.rem(i + 1, NY)
+        k = lax.rem(i + 1 - t * (2 * i - 2), NY)
         weigh(k)
 
         @pl.when(i == 0)
@@ -453,16 +453,17 @@
     loads[4].wait()
     halves[3].wait_recv()
     def part(k):
-        ys = row_chip(k)
+        ys = y if k is None else row_chip(k)
         weights = wo[ys // 2, pl.ds(pl.multiple_of(lax.rem(ys, 2) * 256, 256), 256), :]
-        piece = att_out[0] if k == 0 else att_all[k]
+        piece = att_out[0] if k is None else att_all[k]
         return jnp.dot(piece, weights, preferred_element_type=F32)
 
-    for k in (1, 2):
-        give_back(k).wait_recv()
-    acc[...] = part(0) + part(3) + part(2)
-    give_back(3).wait_recv()
-    projected = acc[...] + part(1)
+    early, late = 3 - 2 * t, 1 + 2 * t
+    for k in (early, 2):
+        give_back(NY - k).wait_recv()
+    acc[...] = part(None) + part(early) + part(2)
+    give_back(NY - late).wait_recv()
+    projected = acc[...] + part(late)
     square = jnp.mean(projected * projected, axis=-1, keepdims=True)
     out_ref[...] = (projected * lax.rsqrt(square + EPSILON)).astype(BF)
 

time: 53.4 us -> 54.1 us (1.013)
  Pallas kernels: 50.1 us -> 50.8 us
    pallas_call x1, Pallas kernels: 50.1 us -> 50.8 us  [shards(): pl.pallas_call(kernel, out_shape=(jax.ShapeDtypeStruct((rows, width), BF)...]
where the time goes in v7:
time: 54.1 us; the launch traced here: 54 us
  Pallas kernels  50.8 us (94%)
  local copies, waits for them, and re-layouts  2.48 us (5%)
  between operations  0.65 us (1%)
    pallas_call x1, Pallas kernels, shards(): pl.pallas_call(kernel, out_shape=(jax.ShapeDtypeStruct((rows, width), BF)...  50.8 us
    unnamed x4, local copies, waits for them, and re-layouts  2.48 us

profile of v7, /device:TPU:1, one launch (start us, length us, event | category | flops | bytes accessed | tf_op | source)
XLA Modules:
  0.0 54.0 jit_solution(9035142675915209395)
XLA Ops:
  0.6 50.8 %shard_map.113 = (bf16[256,1024]{1,0:T(8,128)(2,1)}, f32[8,512]{1,0:T(8,128)}) custom-call(f32[256,128]{1,0:T(8,128)} %constant.8.clone.cr_hbm, f32[256,128]{1,0:T(8,128)} %constant.9.clone.sr_hbm, f32[64,128]{1,0:T(8,128)} %constant.10.clone.cb_hbm, f32[64,128]{1,0:T(8,128)} %constant.11.clone.sb_hbm, bf16[256,1024]{1,0:T(8,128)(2,1)} %bitcast.7, ...), custom_call_target="tpu_custom_call" | custom-call | tf_op jit(solution)/shard_map/pallas_call | solution.py:506
  51.5 0.0 copy-start
  51.5 1.9 %copy.14 = bf16[1,256,1024]{2,1,0:T(8,128)(2,1)} copy(bf16[1,256,1024]{2,1,0:T(8,128)(2,1)} %bitcast.6) | data formatting | bytes 1048576
  53.4 0.0 copy-done
  53.4 0.6 %copy.15 = f32[1,512,8]{1,2,0:T(8,128)} copy(f32[1,512,8]{1,2,0:T(8,128)S(1)} %bitcast.8) | data formatting | bytes 32768
Async XLA Ops:
  51.5 1.9 %copy-start = (f32[8,512]{1,0:T(8,128)S(1)}, f32[8,512]{1,0:T(8,128)}, u32[]{:S(2)}) copy-start(f32[8,512]{1,0:T(8,128)} %get-tuple-element.5) | copy-start | bytes 49156

commit v8 on v6

--- a/solution.py
+++ b/solution.py
@@ -65,6 +65,17 @@
             device_id={"kv": kv_to, "tp": tp_to}, device_id_type=MESH,
         )
 
+    barrier = pltpu.get_barrier_semaphore()
+    peers = [(row_peer(k), tt) for k in range(1, NY) for tt in (t, other)]
+    peers += [(kv, other)]
+    z_up = lax.rem(z + 1, NZ) * NY + y
+    z_dn = lax.rem(z + NZ - 1, NZ) * NY + y
+    peers += [(z_up, t), (z_dn, t)]
+    for kv_to, tp_to in peers:
+        pl.semaphore_signal(
+            barrier, inc=1, device_id={"kv": kv_to, "tp": tp_to}, device_id_type=MESH
+        )
+
     loads = [
         pltpu.make_async_copy(tok_hbm, tok, load_sem.at[0]),
         pltpu.make_async_copy(wk_hbm, wk.at[t], load_sem.at[1]),
@@ -81,17 +92,6 @@
     own_picks = pltpu.make_async_copy(ch_hbm, ch_all.at[0], load_sem.at[12])
     for load in loads[:3] + tables + loads[3:] + [own_picks]:
         load.start()
-
-    barrier = pltpu.get_barrier_semaphore()
-    peers = [(row_peer(k), tt) for k in range(1, NY) for tt in (t, other)]
-    peers += [(kv, other)]
-    z_up = lax.rem(z + 1, NZ) * NY + y
-    z_dn = lax.rem(z + NZ - 1, NZ) * NY + y
-    peers += [(z_up, t), (z_dn, t)]
-    for kv_to, tp_to in peers:
-        pl.semaphore_signal(
-            barrier, inc=1, device_id={"kv": kv_to, "tp": tp_to}, device_id_type=MESH
-        )
 
     left = lax.broadcasted_iota(jnp.int32, (BLK, 128), 1) < BLK
     left_half = lax.broadcasted_iota(jnp.int32, (BLK // 2, 128), 1) < BLK
@@ -235,6 +235,7 @@
     loads[3].wait()
     for copy in halves[2:] + picks:
         copy.start()
+    project_q(t)
     halves[0].wait_recv()
     project_k(other)
     send_heads(key_to_owner, other)
@@ -266,7 +267,6 @@
     for k in (1, 3, 2):
         from_row(v_all, v_own, vy_send, vy_recv, k)
         begin(v_ring, k)
-    project_q(t)
     halves[2].wait_recv()
     project_q(other)
     own_q = pltpu.make_async_copy(qs.at[y], q_all.at[0], load_sem.at[6])

time: 53.4 us -> 53.4 us (level)
  no operation moved by 1% of the time
where the time goes in v8:
time: 53.4 us; the launch traced here: 53.3 us
  Pallas kernels  50.2 us (94%)
  local copies, waits for them, and re-layouts  2.48 us (5%)
  between operations  0.65 us (1%)
    pallas_call x1, Pallas kernels, shards(): pl.pallas_call(kernel, out_shape=(jax.ShapeDtypeStruct((rows, width), BF)...  50.2 us
    unnamed x4, local copies, waits for them, and re-layouts  2.48 us

profile of v8, /device:TPU:1, one launch (start us, length us, event | category | flops | bytes accessed | tf_op | source)
XLA Modules:
  0.0 53.3 jit_solution(10422912633870568451)
XLA Ops:
  0.6 50.2 %shard_map.113 = (bf16[256,1024]{1,0:T(8,128)(2,1)}, f32[8,512]{1,0:T(8,128)}) custom-call(f32[256,128]{1,0:T(8,128)} %constant.8.clone.cr_hbm, f32[256,128]{1,0:T(8,128)} %constant.9.clone.sr_hbm, f32[64,128]{1,0:T(8,128)} %constant.10.clone.cb_hbm, f32[64,128]{1,0:T(8,128)} %constant.11.clone.sb_hbm, bf16[256,1024]{1,0:T(8,128)(2,1)} %bitcast.7, ...), custom_call_target="tpu_custom_call" | custom-call | tf_op jit(solution)/shard_map/pallas_call | solution.py:505
  50.9 0.0 copy-start
  50.9 1.9 %copy.14 = bf16[1,256,1024]{2,1,0:T(8,128)(2,1)} copy(bf16[1,256,1024]{2,1,0:T(8,128)(2,1)} %bitcast.6) | data formatting | bytes 1048576
  52.7 0.0 copy-done
  52.7 0.6 %copy.15 = f32[1,512,8]{1,2,0:T(8,128)} copy(f32[1,512,8]{1,2,0:T(8,128)S(1)} %bitcast.8) | data formatting | bytes 32768
Async XLA Ops:
  50.9 1.9 %copy-start = (f32[8,512]{1,0:T(8,128)S(1)}, f32[8,512]{1,0:T(8,128)}, u32[]{:S(2)}) copy-start(f32[8,512]{1,0:T(8,128)} %get-tuple-element.5) | copy-start | bytes 49156

commit v9 on v6

--- a/solution.py
+++ b/solution.py
@@ -354,22 +354,22 @@
         return top
 
     def softmax(state, half):
-        k, jb, top, bias, total = state
+        k, slab, jb, top, bias, total = state
         for j in range(half * 8, half * 8 + 8):
             shift = top if j == PICK else top - bias[j]
             p = jnp.exp2((scores[jb % 2, j * BLK : j * BLK + BLK, :] - shift) * EXPONENT)
             part = eight(p, jnp.sum)
             total = part if total is None else total + part
-            probs[jb, j * BLK : j * BLK + BLK, :] = p.astype(BF)
+            probs[slab * 4 + jb, j * BLK : j * BLK + BLK, :] = p.astype(BF)
         if half == 1:
             total = jnp.sum(total, axis=0, keepdims=True)
             inverse[k, pl.ds(jb, 1), :] = 1.0 / total
             logsum = top * HEAD_DIM**-0.5 + jnp.log(total)
             for h in range(4):
                 ls_out[k, pl.ds(h, 1), jb * BLK : jb * BLK + BLK] = logsum[:, h * BLK : h * BLK + BLK]
-        return k, jb, top, bias, total
-
-    def weigh(k):
+        return k, slab, jb, top, bias, total
+
+    def weigh(k, slab):
         state = None
         for jb in range(4):
             bias = gather_keys(k, jb)
@@ -380,7 +380,7 @@
                 if state is not None:
                     state = softmax(state, half)
             top = jnp.max(jnp.maximum(*tops), axis=0, keepdims=True)
-            state = (k, jb, top, bias, None)
+            state = (k, slab, jb, top, bias, None)
         for half in range(2):
             state = softmax(state, half)
 
@@ -400,11 +400,11 @@
                 vt[jb, half_blk:, columns] = high.astype(BF)
             previous = block
 
-    def combine(k):
+    def combine(k, slab):
         for jb in range(4):
             gather_values(k, jb)
         mixed = [
-            jnp.dot(vt[jb], probs[jb], preferred_element_type=F32) for jb in range(4)
+            jnp.dot(vt[jb], probs[slab * 4 + jb], preferred_element_type=F32) for jb in range(4)
         ]
         for jb in range(4):
             turned_back = (mixed[jb] * inverse[k, pl.ds(jb, 1), :]).T
@@ -426,23 +426,31 @@
 
     @pl.loop(0, NY)
     def _(i):
-        k = lax.rem(i + 1, NY)
-        weigh(k)
+        weigh(lax.rem(i + 1, NY), lax.rem(i, 2))
 
         @pl.when(i == 0)
         def _():
             for r in order:
                 step(v_ring, NZ // 2, r)
+
+        @pl.when(i == 1)
+        def _():
             for rel in range(NZ):
                 for r in range(NY):
                     v_ring[2](rel, r).wait_recv()
 
-        combine(k)
-
-        @pl.when(k > 0)
-        def _():
-            give_back(k).start()
-            log_piece(k).start()
+        ready_from = jnp.where(i == 1, 0, i)
+        ready_to = jnp.where(i == 0, 0, i + 1)
+
+        @pl.loop(ready_from, ready_to)
+        def _(g):
+            k = lax.rem(g + 1, NY)
+            combine(k, lax.rem(g, 2))
+
+            @pl.when(k > 0)
+            def _():
+                give_back(k).start()
+                log_piece(k).start()
 
     pl.when(jnp.logical_not(to_self))(lambda: log_piece(0).start())
 
@@ -533,7 +541,7 @@
             pltpu.VMEM((2, (PICK + 1) * BLK, 128), BF),
             pltpu.VMEM((4, BLK, (PICK + 1) * BLK), BF),
             pltpu.VMEM((2, (PICK + 1) * BLK, 4 * BLK), F32),
-            pltpu.VMEM((4, (PICK + 1) * BLK, 4 * BLK), BF),
+            pltpu.VMEM((8, (PICK + 1) * BLK, 4 * BLK), BF),
             pltpu.VMEM((NY, 4, 4 * BLK), F32),
             pltpu.VMEM((NY, rows, 256), BF),
             pltpu.VMEM((NY, rows, 256), BF),

time: 53.4 us -> 54.7 us (1.024)
  Pallas kernels: 50.1 us -> 51.5 us
    pallas_call x1, Pallas kernels: 50.1 us -> 51.5 us  [shards(): pl.pallas_call(kernel, out_shape=(jax.ShapeDtypeStruct((rows, width), BF)...]
where the time goes in v9:
time: 54.7 us; the launch traced here: 54.6 us
  Pallas kernels  51.5 us (94%)
  local copies, waits for them, and re-layouts  2.48 us (5%)
  between operations  0.65 us (1%)
    pallas_call x1, Pallas kernels, shards(): pl.pallas_call(kernel, out_shape=(jax.ShapeDtypeStruct((rows, width), BF)...  51.5 us
    unnamed x4, local copies, waits for them, and re-layouts  2.48 us

profile of v9, /device:TPU:1, one launch (start us, length us, event | category | flops | bytes accessed | tf_op | source)
XLA Modules:
  0.0 54.6 jit_solution(16142994511248425129)
XLA Ops:
  0.6 51.5 %shard_map.113 = (bf16[256,1024]{1,0:T(8,128)(2,1)}, f32[8,512]{1,0:T(8,128)}) custom-call(f32[256,128]{1,0:T(8,128)} %constant.8.clone.cr_hbm, f32[256,128]{1,0:T(8,128)} %constant.9.clone.sr_hbm, f32[64,128]{1,0:T(8,128)} %constant.10.clone.cb_hbm, f32[64,128]{1,0:T(8,128)} %constant.11.clone.sb_hbm, bf16[256,1024]{1,0:T(8,128)(2,1)} %bitcast.7, ...), custom_call_target="tpu_custom_call" | custom-call | tf_op jit(solution)/shard_map/pallas_call | solution.py:513
  52.1 0.0 copy-start
  52.2 1.9 %copy.14 = bf16[1,256,1024]{2,1,0:T(8,128)(2,1)} copy(bf16[1,256,1024]{2,1,0:T(8,128)(2,1)} %bitcast.6) | data formatting | bytes 1048576
  54.0 0.0 copy-done
  54.0 0.6 %copy.15 = f32[1,512,8]{1,2,0:T(8,128)} copy(f32[1,512,8]{1,2,0:T(8,128)S(1)} %bitcast.8) | data formatting | bytes 32768
Async XLA Ops:
  52.1 1.9 %copy-start = (f32[8,512]{1,0:T(8,128)S(1)}, f32[8,512]{1,0:T(8,128)}, u32[]{:S(2)}) copy-start(f32[8,512]{1,0:T(8,128)} %get-tuple-element.5) | copy-start | bytes 49156
